TPU v7x, 256 devices: a 4x2x16 block of a 4x16x16 slice. The times are simulated.
256 devices in a mesh: grp: 2 (over y), sp: 32 (over z, core), tp: 4 (over x).
Axes of the slice: x: 4, y: 2, z: 16, core: 2. Of those that a mesh axis runs over, the one named last changes fastest.
The devices are a block of a 4x16x16 slice.
Arguments:
- residual: bfloat16 [49152, 2048], P(('grp', 'sp', 'tp')), parts along dimension 0, may hold values from -6 to 6
- value_projected: bfloat16 [49152, 4096], P(('grp', 'sp'), 'tp'), parts along dimension 0, may hold values from -6 to 6
- gate_projected: bfloat16 [49152, 4096], P(('grp', 'sp'), 'tp'), parts along dimension 0, may hold values from -6 to 6
- wide_key_rows: bfloat16 [49152, 1024], P(('grp', 'sp'), 'tp'), parts along dimension 0, may hold values from -6 to 6
- wide_query_rows: bfloat16 [49152, 1024], P(('grp', 'sp'), 'tp'), parts along dimension 0, may hold values from -6 to 6
- narrow_key_rows: bfloat16 [49152, 512], P(('grp', 'sp'), 'tp'), parts along dimension 0, may hold values from -6 to 6
- narrow_query_rows: bfloat16 [49152, 512], P(('grp', 'sp'), 'tp'), parts along dimension 0, may hold values from -6 to 6
- step_before_softplus: float32 [49152, 64], P(('grp', 'sp'), 'tp'), parts along dimension 0, may hold values from -5 to 5
- extra_log_decay: float32 [49152, 64], P(('grp', 'sp'), 'tp'), parts along dimension 0, may hold values from -0.7 to 0
- log_decay_rate: float32 [64], P('tp'), may hold values from -12.3 to -2.99
- value_kernel: bfloat16 [4, 4096], P(None, 'tp'), may hold values from -3 to 3
- wide_key_kernel: bfloat16 [4, 1024], P(None, 'tp'), may hold values from -3 to 3
- wide_query_kernel: bfloat16 [4, 1024], P(None, 'tp'), may hold values from -3 to 3
- narrow_key_kernel: bfloat16 [4, 512], P(None, 'tp'), may hold values from -3 to 3
- narrow_query_kernel: bfloat16 [4, 512], P(None, 'tp'), may hold values from -3 to 3
- head_norm_gain: bfloat16 [4096], P('tp'), may hold values from 0.099609375 to 1.8984375
- output_matrix: bfloat16 [4096, 2048], P('tp'), may hold values from -0.09375 to 0.09375
- feedforward_norm_gain: bfloat16 [2048], replicated, may hold values from 0.099609375 to 1.8984375
- gate_matrix: bfloat16 [2048, 3072], P('sp', 'tp'), may hold values from -0.125 to 0.125
- up_matrix: bfloat16 [2048, 3072], P('sp', 'tp'), may hold values from -0.125 to 0.125
- down_matrix: bfloat16 [2048, 3072], P('sp', 'tp'), may hold values from -0.3125 to 0.3125
Outputs:
- mixed: bfloat16 [49152, 2048], P(('grp', 'sp', 'tp')), parts along dimension 0
There are 2 independent parts, one for each index of `grp`. A program takes and returns all parts, laid end to end along the dimension named above; an argument that names none is the same for every part. Nothing has to cross between parts.
All inputs are finite; a program needn't handle non-finite values.
Results may differ from a plain program's by a relative error of at most 0.015.
Values may be sent and summed in bfloat16 or wider, within the bound.
No kernel may reach another device: no remote copies, remote signals or barrier semaphores. Data moves between devices by JAX's collectives and lax.ppermute only.
A program may use at most 128 MiB of HBM per device.

v0:
```python
import functools

import jax
import jax.numpy as jnp
import numpy as np
from jax import lax
from jax.experimental import pallas as pl
from jax.experimental.pallas import tpu as pltpu
from jax.sharding import PartitionSpec as P


CH = 64
PER = 4
GW = PER * CH
BT = 128
WIDE = 128
NARROW = 64
TAPS = 4
EDGE = 8
EPS = 1e-6
F32 = jnp.float32
BF16 = jnp.bfloat16
VMEM_LIMIT = 60 << 20
SMALL_LIMIT = 12 << 20
FEED_LIMIT = 24 << 20


def dot(a, b):
    return jnp.dot(a, b, preferred_element_type=F32)


def dot_nt(a, b):
    return lax.dot_general(a, b, (((1,), (1,)), ((), ())), preferred_element_type=F32)


def dot_tn(a, b):
    return lax.dot_general(a, b, (((0,), (0,)), ((), ())), preferred_element_type=F32)


def halves(x):
    hi = x.astype(BF16)
    return hi, (x - hi.astype(F32)).astype(BF16)


def dot2(pair, b):
    return dot(pair[0], b) + dot(pair[1], b)


def silu(x):
    h = 0.5 * x
    return h + h * jnp.tanh(h)


def group_rows(groups):
    out, row = [], 0
    wide_cols = (groups // 2) * WIDE
    for g in range(groups):
        size = NARROW if g % 2 else WIDE
        key = wide_cols + (g // 2) * NARROW if g % 2 else (g // 2) * WIDE
        out.append((row, size, key))
        row += size
    return out, row


def conv_cols(buf, cols, ker):
    k = ker.astype(F32)
    first = EDGE - TAPS + 1
    total = buf[first : first + BT, cols] * k[0:1]
    for tap in range(1, TAPS):
        total += buf[first + tap : first + tap + BT, cols] * k[tap : tap + 1]
    return silu(total)


def edge_kernel(*refs):
    ins, (edge, both) = refs[:-2], refs[-2:]
    at = 0
    for part in ins[:-3]:
        edge[:, at : at + part.shape[1]] = part[...]
        at += part.shape[1]
    at = 0
    for part in ins[-3:]:
        both[:, at : at + part.shape[1]] = part[...]
        at += part.shape[1]


def states_kernel(
    groups, chunk, rim, value, wk, nk, step, extra, rate, kv, kwk, knk, table, place, pick,
    up, kk, er, eR, hs, st, bufv, bufk, state, before,
):
    i = pl.program_id(0)
    info, _ = group_rows(groups)
    inner, wcols, ncols = value.shape[1], wk.shape[1], nk.shape[1]

    @pl.when(i == 0)
    def _():
        bufv[0:EDGE, :] = rim[:, 0:inner].astype(F32)
        bufk[0:EDGE, :] = rim[:, inner : inner + wcols + ncols].astype(F32)
        state[...] = jnp.zeros_like(state)
        before[...] = jnp.zeros_like(before)

    bufv[EDGE:, :] = value[...].astype(F32)
    bufk[EDGE:, 0:wcols] = wk[...].astype(F32)
    bufk[EDGE:, wcols:] = nk[...].astype(F32)

    heads = step.shape[0]
    diagonal = lax.broadcasted_iota(jnp.int32, (heads, heads), 0) == lax.broadcasted_iota(
        jnp.int32, (heads, heads), 1
    )
    speed = jnp.exp(jnp.sum(jnp.where(diagonal, rate[...], 0.0), axis=1, keepdims=True))
    dt = jnp.log(1.0 + jnp.exp(step[...]))
    a = extra[...] - speed * dt
    upto = lax.broadcasted_iota(jnp.int32, (BT, BT), 0) <= lax.broadcasted_iota(
        jnp.int32, (BT, BT), 1
    )
    upto = jnp.where(upto, 1.0, 0.0).astype(BF16)
    a1 = a.astype(BF16)
    a2, a3 = halves(a - a1.astype(F32))
    r = dot(a1, upto) + dot(a2, upto) + dot(a3, upto)
    mid, end = r[:, BT // 2 - 1 : BT // 2], r[:, BT - 1 : BT]
    er[...] = jnp.exp(r - mid).T
    eR[...] = jnp.exp(r + before[...]).T
    before[...] = before[...] + end
    inward = halves((jnp.exp(mid - r) * dt).T)
    lane = lax.broadcasted_iota(jnp.int32, r.shape, 1)
    scales = jnp.exp(jnp.where(lane == 0, mid, jnp.where(lane == 1, end, end - mid)))
    scales = halves(scales.T[0:8])

    for c in range(0, wcols, 128):
        cols = slice(c, c + 128)
        kk[:, cols] = conv_cols(bufk, cols, kwk[:, cols]).astype(BF16)
    for c in range(0, ncols, 128):
        cols = slice(wcols + c, wcols + c + 128)
        kk[:, cols] = conv_cols(bufk, cols, knk[:, c : c + 128]).astype(BF16)
    for g, (row, size, key) in enumerate(info):
        cols = slice(g * GW, (g + 1) * GW)
        tab = table[:, cols]
        f = dot2(inward, tab)
        s = dot2(scales, tab)
        u = conv_cols(bufv, cols, kv[:, cols]).astype(BF16).astype(F32)
        scaled = (u * f).astype(BF16)
        up[:, cols] = scaled
        added = dot_tn(kk[:, key : key + size], scaled)
        old = state[row : row + size, :]
        hs[0, row : row + size, :] = (old * s[0:1]).astype(BF16)
        state[row : row + size, :] = old * s[1:2] + added * s[2:3]
    bufv[0:EDGE, :] = bufv[BT:, :]
    bufk[0:EDGE, :] = bufk[BT:, :]

    @pl.when(i == pl.num_programs(0) - 1)
    def _():
        total = halves(before[...].T[0:8])
        line_t = (dot(total[0], place[:, 0:GW]) + dot(total[1], place[:, GW:]))[0:1]
        sent = dot(pick[...], state[...].astype(BF16))
        used, padded = chunk
        rows = lax.broadcasted_iota(jnp.int32, sent.shape, 0)
        st[...] = jnp.where(rows % padded == used, line_t, sent).astype(BF16)


def inner_kernel(groups, rim, wq, nq, kwq, knq, kk, up, er, hs, table, yl, qq, bufq):
    i = pl.program_id(0)
    info, _ = group_rows(groups)
    wcols, ncols = wq.shape[1], nq.shape[1]

    @pl.when(i == 0)
    def _():
        bufq[0:EDGE, :] = rim[:, rim.shape[1] - wcols - ncols :].astype(F32)

    bufq[EDGE:, 0:wcols] = wq[...].astype(F32)
    bufq[EDGE:, wcols:] = nq[...].astype(F32)
    for c in range(0, wcols, 128):
        cols = slice(c, c + 128)
        qq[:, cols] = conv_cols(bufq, cols, kwq[:, cols]).astype(BF16)
    for c in range(0, ncols, 128):
        cols = slice(wcols + c, wcols + c + 128)
        qq[:, cols] = conv_cols(bufq, cols, knq[:, c : c + 128]).astype(BF16)
    bufq[0:EDGE, :] = bufq[BT:, :]
    outward = halves(er[...])
    t = lax.broadcasted_iota(jnp.int32, (BT, BT), 0)
    s = lax.broadcasted_iota(jnp.int32, (BT, BT), 1)
    for g, (row, size, key) in enumerate(info):
        cols = slice(g * GW, (g + 1) * GW)
        q, k = qq[:, key : key + size], kk[:, key : key + size]
        weights = jnp.where(s <= t, dot_nt(q, k), 0.0).astype(BF16)
        y = dot(weights, up[:, cols]) + dot(q, hs[0, row : row + size, :])
        yl[:, cols] = y * dot2(outward, table[:, cols])


def row_fades(groups, used, padded, place, sums, table):
    info, _ = group_rows(groups)
    factor = halves(jnp.exp(sums))
    fades = [dot2(factor, table[:, g * GW : (g + 1) * GW]) for g in range(groups)]
    row = lax.broadcasted_iota(jnp.int32, (padded, GW), 0) + place * used
    masks = [row >= info[g][0] for g in range(1, groups)]

    def fade(k):
        out = jnp.broadcast_to(fades[0][k : k + 1], (padded, GW))
        for g in range(1, groups):
            out = jnp.where(masks[g - 1], fades[g][k : k + 1], out)
        return out

    return fade


def near_kernel(groups, chunk, where_ref, got, gather, unplace, place, table, prefix, sums, sent):
    used, padded = chunk
    count = got.shape[0] // padded
    lines = dot(gather[...], got[...]).astype(BF16)
    logs = dot(lines, unplace[...])
    sums[...] = logs
    fade = row_fades(groups, used, padded, where_ref[0], logs, table)
    held = jnp.zeros((padded, GW), F32)
    for k in range(count):
        part = slice(k * padded, (k + 1) * padded)
        prefix[part, :] = held
        held = fade(k) * held + got[part, :].astype(F32)
    total = halves(jnp.broadcast_to(jnp.sum(logs, axis=0, keepdims=True), (8, logs.shape[1])))
    line = (dot(total[0], place[:, 0:GW]) + dot(total[1], place[:, GW:]))[0:1]
    row = lax.broadcasted_iota(jnp.int32, held.shape, 0)
    sent[...] = jnp.where(row == used, line, held).astype(BF16)


def far_kernel(groups, chunk, where_ref, prefix, sums, unplace, table, *refs):
    used, padded = chunk
    others, out = refs[:-1], refs[-1]
    count = prefix.shape[0] // padded
    so_far = jnp.zeros((8, sums.shape[1]), F32)
    entering = jnp.zeros((padded, GW), F32)
    for n, other in enumerate(others):
        part = other[...].astype(F32)
        if n > 0:
            part = part * row_fades(groups, used, padded, where_ref[0], so_far, table)(0)
        entering += part
        so_far += dot(other[used : used + 8, :], unplace[...])[0:1]
    fade = row_fades(groups, used, padded, where_ref[0], sums[...], table)
    for k in range(count):
        part = slice(k * padded, (k + 1) * padded)
        out[part, :] = (prefix[part, :] + entering).astype(BF16)
        entering = fade(k) * entering


def project_kernel(groups, count, _, *refs):
    ins, (hin, gain, matrix, table, table_t) = refs[: 4 * count], refs[4 * count : 4 * count + 5]
    outs, (held, normed) = refs[4 * count + 5 : -2], refs[-2:]
    info, _ = group_rows(groups)
    share = ins[0].shape[0]

    @pl.when(pl.program_id(0) == 0)
    def _():
        for n in range(count):
            yl, qq, eR, gate = ins[4 * n : 4 * n + 4]
            reach = halves(eR[...])
            squares = jnp.zeros((share, table.shape[0]), F32)
            for g, (row, size, key) in enumerate(info):
                cols = slice(g * GW, (g + 1) * GW)
                outer = dot(qq[:, key : key + size], hin[row : row + size, :])
                y = yl[:, cols] + outer * dot2(reach, table[:, cols])
                gated = y * silu(gate[:, cols].astype(F32))
                held[:, cols] = gated
                squares += dot2(halves(gated * gated), table_t[cols, :])
            scale = halves(lax.rsqrt(squares * (1.0 / CH) + EPS))
            for g in range(groups):
                cols = slice(g * GW, (g + 1) * GW)
                unit = held[:, cols] * dot2(scale, table[:, cols]) * gain[:, cols].astype(F32)
                normed[n * share : (n + 1) * share, cols] = unit.astype(BF16)

    p = dot(normed[...], matrix[...]).astype(BF16)
    half = outs[0].shape[0]
    for n, out in enumerate(outs):
        out[...] = p[n * half : (n + 1) * half]


def place_kernel(unpick, back, out):
    out[...] = dot(unpick[...], back[...]).astype(BF16)


def norm_kernel(res, own, one, two, gain, after, x):
    total = own[...].astype(F32) + one[...].astype(F32) + two[...].astype(F32)
    mixed = (res[...].astype(F32) + total).astype(BF16)
    after[...] = mixed
    rows = mixed.astype(F32)
    scale = lax.rsqrt(jnp.mean(rows * rows, axis=1, keepdims=True) + EPS)
    x[...] = (rows * scale * gain[...].astype(F32)).astype(BF16)


def last_kernel(own_t, t1, t2, after_t, own_b, b1, b2, after_b, out):
    half = own_t.shape[0]
    for at, (own, one, two, after) in (
        (0, (own_t, t1, t2, after_t)),
        (half, (own_b, b1, b2, after_b)),
    ):
        total = own[...].astype(F32) + one[...].astype(F32) + two[...].astype(F32)
        out[at : at + half, :] = (after[...].astype(F32) + 0.5 * total).astype(BF16)


def pair_kernel(one, two, out):
    out[...] = (one[...].astype(F32) + two[...].astype(F32)).astype(BF16)


def feed_kernel(count, *refs):
    xs, (gate, up, down) = refs[:count], refs[count : count + 3]
    outs, total = refs[count + 3 : 2 * count + 3], refs[2 * count + 3]
    j = pl.program_id(0)
    x = jnp.concatenate([r[...] for r in xs], axis=0) if count > 1 else xs[0][...]
    hidden = (silu(dot(x, gate[...])) * dot(x, up[...])).astype(BF16)
    added = dot_nt(hidden, down[...])

    @pl.when(j == 0)
    def _():
        total[...] = added

    @pl.when(j > 0)
    def _():
        total[...] = total[...] + added

    @pl.when(j == pl.num_programs(0) - 1)
    def _():
        half = xs[0].shape[0]
        for n, out in enumerate(outs):
            out[...] = total[n * half : (n + 1) * half, :].astype(BF16)


def params(limit=VMEM_LIMIT):
    return pltpu.CompilerParams(dimension_semantics=("arbitrary",), vmem_limit_bytes=limit)


def cost(flops, moved):
    return pl.CostEstimate(flops=int(flops), bytes_accessed=int(moved), transcendentals=0)


def fixed(a):
    return pl.BlockSpec(a.shape, lambda *_: (0,) * a.ndim)


def whole(kernel, out_shapes, *args, flops=2e8):
    return pl.pallas_call(
        kernel,
        out_shape=out_shapes,
        compiler_params=pltpu.CompilerParams(vmem_limit_bytes=SMALL_LIMIT),
        cost_estimate=cost(flops, sum(a.size * 2 for a in args)),
    )(*args)


def ring(value, axis, step):
    count = lax.axis_size(axis)
    return lax.ppermute(value, axis, [(i, (i + step) % count) for i in range(count)])


def feed(xs, weights, tile=256):
    half, width = xs[0].shape
    inner = weights.shape[1] // 3
    tiles = inner // tile
    rows = half * len(xs)
    shape = jax.ShapeDtypeStruct((half, width), BF16)
    part = lambda n: pl.BlockSpec((width, tile), lambda j: (0, n * tiles + j))
    return pl.pallas_call(
        functools.partial(feed_kernel, len(xs)),
        grid=(tiles,),
        in_specs=[fixed(a) for a in xs] + [part(0), part(1), part(2)],
        out_specs=[pl.BlockSpec((half, width), lambda j: (0, 0))] * len(xs),
        out_shape=[shape] * len(xs),
        scratch_shapes=[pltpu.VMEM((rows, width), F32)],
        compiler_params=params(FEED_LIMIT),
        cost_estimate=cost(6 * rows * width * inner, weights.size * 2),
    )(*xs, weights, weights, weights)


def collect(own, left, right, opposite):
    send = lambda value, step: ring(value, "tp", step)
    from_left = send(opposite[0], 1)
    from_right = send(opposite[1], -1)
    bottom_left = send(right[1], 1)
    top_right = send(left[0], -1)
    shape = jax.ShapeDtypeStruct(own[0].shape, BF16)
    to_right = whole(pair_kernel, shape, right[0], from_left)
    to_left = whole(pair_kernel, shape, left[1], from_right)
    top_left = send(to_right, 1)
    bottom_right = send(to_left, -1)
    return (own[0], top_left, top_right), (own[1], bottom_left, bottom_right)


def on_device(
    residual, value_projected, gate_projected, wide_key_rows, wide_query_rows, narrow_key_rows,
    narrow_query_rows, step_before_softplus, extra_log_decay, log_decay_rate, value_kernel,
    wide_key_kernel, wide_query_kernel, narrow_key_kernel, narrow_query_kernel, head_norm_gain,
    output_matrix, feedforward_norm_gain, gate_matrix, up_matrix, down_matrix,
):
    sp, tp = lax.axis_size("sp"), lax.axis_size("tp")
    length, inner = value_projected.shape
    heads = inner // CH
    groups = heads // PER
    wcols, ncols = wide_key_rows.shape[1], narrow_key_rows.shape[1]
    keys = wcols + ncols
    width = output_matrix.shape[1]
    _, rows = group_rows(groups)
    near = 8 if sp % 8 == 0 else 2
    used = rows // near
    padded = -(-(used + 8) // 16) * 16
    chunk = (used, padded)
    blocks = length // BT
    me_sp, me_tp = lax.axis_index("sp"), lax.axis_index("tp")

    struct = jax.ShapeDtypeStruct
    table_np = (np.arange(heads)[:, None] == np.arange(inner)[None] // CH).astype(np.float32)
    table, table_t = jnp.asarray(table_np, BF16), jnp.asarray(table_np.T, BF16)
    place_np = np.zeros((heads, 2 * GW), np.float32)
    place_np[np.arange(heads), np.arange(heads)] = 1
    place_np[np.arange(heads), GW + heads + np.arange(heads)] = 1
    unplace_np = (place_np[:, :GW] + place_np[:, GW:]).T
    place, unplace = jnp.asarray(place_np, BF16), jnp.asarray(unplace_np, BF16)
    slot = np.arange(near * padded)
    pick_np = (
        (slot % padded < used)[:, None]
        & ((slot // padded * used + slot % padded)[:, None] == np.arange(rows)[None])
    ).astype(np.float32)
    pick, unpick = jnp.asarray(pick_np, BF16), jnp.asarray(pick_np.T, BF16)
    gather = jnp.asarray(
        (np.arange(near)[:, None] * padded + used == slot[None]).astype(np.float32), BF16
    )

    rowed = (
        value_projected, wide_key_rows, narrow_key_rows, wide_query_rows, narrow_query_rows
    )
    span = sum(a.shape[1] for a in rowed)
    mats = (gate_matrix, up_matrix, down_matrix)
    edge, weights = pl.pallas_call(
        edge_kernel,
        grid=(1,),
        in_specs=[
            pl.BlockSpec((EDGE, a.shape[1]), lambda i: (length // EDGE - 1, 0)) for a in rowed
        ]
        + [fixed(a) for a in mats],
        out_specs=[
            pl.BlockSpec((EDGE, span), lambda i: (0, 0)),
            pl.BlockSpec((mats[0].shape[0], 3 * mats[0].shape[1]), lambda i: (0, 0)),
        ],
        out_shape=[
            struct((EDGE, span), BF16),
            struct((mats[0].shape[0], 3 * mats[0].shape[1]), BF16),
        ],
        compiler_params=params(),
        cost_estimate=cost(1e6, 1e6),
    )(*rowed, *mats)
    rim = lax.ppermute(edge, "sp", [(i, i + 1) for i in range(sp - 1)])

    gain, ff_gain = head_norm_gain.reshape(1, inner), feedforward_norm_gain.reshape(1, width)
    rim, gain, ff_gain = lax.optimization_barrier((rim, gain, ff_gain))
    row_spec = lambda w: pl.BlockSpec((BT, w), lambda i: (i, 0))
    time_spec = pl.BlockSpec((heads, BT), lambda i: (0, i))
    rate = log_decay_rate.reshape(1, heads)
    up, kk, er, eR, hs, st = pl.pallas_call(
        functools.partial(states_kernel, groups, chunk),
        grid=(blocks,),
        in_specs=[
            fixed(rim), row_spec(inner), row_spec(wcols), row_spec(ncols), time_spec,
            time_spec, fixed(rate), fixed(value_kernel), fixed(wide_key_kernel),
            fixed(narrow_key_kernel), fixed(table), fixed(place), fixed(pick),
        ],
        out_specs=[
            row_spec(inner), row_spec(keys), row_spec(heads), row_spec(heads),
            pl.BlockSpec((1, rows, GW), lambda i: (i, 0, 0)),
            pl.BlockSpec((near * padded, GW), lambda i: (0, 0)),
        ],
        out_shape=[
            struct((length, inner), BF16), struct((length, keys), BF16),
            struct((length, heads), F32), struct((length, heads), F32),
            struct((blocks, rows, GW), BF16), struct((near * padded, GW), BF16),
        ],
        scratch_shapes=[
            pltpu.VMEM((EDGE + BT, inner), F32), pltpu.VMEM((EDGE + BT, keys), F32),
            pltpu.VMEM((rows, GW), F32), pltpu.VMEM((heads, BT), F32),
        ],
        compiler_params=params(),
        cost_estimate=cost(8e9, 6e6),
    )(
        rim, value_projected, wide_key_rows, narrow_key_rows, step_before_softplus.T,
        extra_log_decay.T, rate, value_kernel, wide_key_kernel, narrow_key_kernel, table, place,
        pick,
    )

    seats = [[q + n for n in range(near)] for q in range(0, sp, near)]
    exchange = lambda a: lax.all_to_all(a, "sp", 0, 0, axis_index_groups=seats, tiled=True)
    got = exchange(st)
    yl, qq = pl.pallas_call(
        functools.partial(inner_kernel, groups),
        grid=(blocks,),
        in_specs=[
            fixed(rim), row_spec(wcols), row_spec(ncols), fixed(wide_query_kernel),
            fixed(narrow_query_kernel), row_spec(keys), row_spec(inner), row_spec(heads),
            pl.BlockSpec((1, rows, GW), lambda i: (i, 0, 0)), fixed(table),
        ],
        out_specs=[row_spec(inner), row_spec(keys)],
        out_shape=[struct((length, inner), F32), struct((length, keys), BF16)],
        scratch_shapes=[pltpu.VMEM((EDGE + BT, keys), F32)],
        compiler_params=params(),
        cost_estimate=cost(8e9, 6e6),
    )(
        rim, wide_query_rows, narrow_query_rows, wide_query_kernel, narrow_query_kernel, kk, up,
        er, hs, table,
    )
    got, yl = lax.optimization_barrier((got, yl))
    far = [
        pltpu.with_memory_space_constraint(a, pltpu.HBM) for a in (yl, qq, eR, gate_projected, output_matrix)
    ]
    smem = pl.BlockSpec(memory_space=pltpu.SMEM)
    vmem = pl.BlockSpec(memory_space=pltpu.VMEM)
    seat = lax.rem(me_sp, near).reshape(1)
    prefix, sums, sent = pl.pallas_call(
        functools.partial(near_kernel, groups, chunk),
        in_specs=[smem] + [vmem] * 5,
        out_shape=[struct(st.shape, F32), struct((near, heads), F32), struct((padded, GW), BF16)],
        compiler_params=pltpu.CompilerParams(vmem_limit_bytes=SMALL_LIMIT),
        cost_estimate=cost(1e9, 1e6),
    )(seat, got, gather, unplace, place, table)
    others = [
        lax.ppermute(sent, "sp", [(i, i + near * n) for i in range(sp - near * n)])
        for n in range(1, sp // near)
    ]
    weights, *others = lax.optimization_barrier((weights, *others))
    weights = lax.all_gather(weights, "sp", axis=0, tiled=True)
    weights = pltpu.with_memory_space_constraint(weights, pltpu.HBM)
    entered = pl.pallas_call(
        functools.partial(far_kernel, groups, chunk),
        in_specs=[smem] + [vmem] * (4 + len(others)),
        out_shape=struct(st.shape, BF16),
        compiler_params=pltpu.CompilerParams(vmem_limit_bytes=SMALL_LIMIT),
        cost_estimate=cost(1e9, 1e6),
    )(seat, prefix, sums, unplace, table, *others)
    back = exchange(entered)
    hin = whole(place_kernel, struct((rows, GW), BF16), unpick, back)

    share = length // tp
    half = share // 2
    tile = 512

    def project(*offsets):
        count = len(offsets)
        mine = lambda w, n: pl.BlockSpec(
            (share, w), lambda i, me: (lax.rem(me[0] + offsets[n], tp), 0)
        )
        return pl.pallas_call(
            functools.partial(project_kernel, groups, count),
            grid_spec=pltpu.PrefetchScalarGridSpec(
                num_scalar_prefetch=1,
                grid=(width // tile,),
                in_specs=[mine(w, n) for n in range(count) for w in (inner, keys, heads, inner)]
                + [fixed(hin), fixed(gain), pl.BlockSpec((inner, tile), lambda i, o: (0, i))]
                + [fixed(table), fixed(table_t)],
                out_specs=[pl.BlockSpec((half, tile), lambda i, o: (0, i))] * (2 * count),
                scratch_shapes=[
                    pltpu.VMEM((share, inner), F32), pltpu.VMEM((count * share, inner), BF16)
                ],
            ),
            out_shape=[struct((half, width), BF16)] * (2 * count),
            compiler_params=params(FEED_LIMIT),
            cost_estimate=cost(2 * count * share * inner * width, 6e6),
        )(me_tp.reshape(1), *far[:4] * count, hin, gain, far[4], table, table_t)

    opposite, sides, own = project(2), project(1, 3), project(0)
    right, left = sides[:2], sides[2:]
    top, bottom = collect(own, left, right, opposite)
    pair = [struct((half, width), BF16)] * 2

    def norm(at, terms):
        same = pl.BlockSpec((half, width), lambda i: (0, 0))
        return pl.pallas_call(
            norm_kernel,
            grid=(1,),
            in_specs=[pl.BlockSpec((half, width), lambda i: (at, 0))]
            + [same] * 3
            + [fixed(ff_gain)],
            out_specs=[same] * 2,
            out_shape=pair,
            compiler_params=params(SMALL_LIMIT),
            cost_estimate=cost(1e9, 5 * half * width * 2),
        )(residual, *terms, ff_gain)

    (after_t, x_t), (after_b, x_b) = norm(0, top), norm(1, bottom)

    left_t, right_b = ring(x_t, "tp", 1), ring(x_b, "tp", -1)
    left_b, right_t = ring(x_b, "tp", 1), ring(x_t, "tp", -1)
    opp_t, opp_b = ring(left_t, "tp", 1), ring(right_b, "tp", -1)
    own = feed([x_t, x_b], weights)
    near = feed([left_t, left_b, right_t, right_b], weights)
    opposite = feed([opp_t, opp_b], weights)
    top, bottom = collect(own, near[:2], near[2:], opposite)
    return whole(
        last_kernel, struct((share, width), BF16), *top, after_t, *bottom, after_b
    )


def solution(mesh):
    rows = P(("grp", "sp"), "tp")
    in_specs = (P(("grp", "sp", "tp"), None),) + (rows,) * 8 + (P("tp"),) + (P(None, "tp"),) * 5
    in_specs += (P("tp"), P("tp", None), P()) + (P("sp", "tp"),) * 3
    return jax.shard_map(
        on_device,
        mesh=mesh,
        in_specs=in_specs,
        out_specs=P(("grp", "sp", "tp"), None),
        check_vma=False,
    )
```

profile of v0, /device:TPU:38, one launch (start us, length us, event | category | flops | bytes accessed | tf_op | source)
XLA Modules:
  0.0 200.5 jit_solution(7169298029826203908)
XLA Ops:
  6.6 1.8 shard_map.262
  8.4 1.8 collective-permute-start
  11.9 11.9 %shard_map.263 = (bf16[768,1024]{1,0:T(8,128)(2,1)}, bf16[768,384]{1,0:T(8,128)(2,1)}, f32[768,16]{1,0:T(8,128)}, f32[768,16]{1,0:T(8,128)}, bf16[6,384,256]{2,1,0:T(8,128)(2,1)}, /*index=5*/bf16[512,256]{1,0:T(8,128)(2,1)}) custom-call(bf16[8,1792]{1,0:T(8,128)(2,1)} %copy-done.11, bf16[768,1024]{1,0:T(8,128)(2,1)} %value.1, bf16[768,256]{1,0:T(8,128)(2,1)} %wk.1, ...), custom_call_target="tpu_custom_call" | custom-call | flops 8000000000 | bytes 6000000 | tf_op jit(solution)/shard_map/pallas_call | solution.py:450
  23.8 12.4 %all-to-all-start = ((bf16[8,64,256]{2,1,0:T(8,128)(2,1)}), bf16[8,64,256]{2,1,0:T(8,128)(2,1)S(1)}, u32[]{:S(2)}, u32[]{:S(2)}) async-start(bf16[8,64,256]{2,1,0:T(8,128)(2,1)} %bitcast.11), calls=%async_computation | async-start | bytes 524288 | tf_op jit(solution)/shard_map/all_to_all | solution.py:481
  36.3 8.0 %shard_map.264 = (f32[768,1024]{1,0:T(8,128)}, bf16[768,384]{1,0:T(8,128)(2,1)}) custom-call(bf16[8,1792]{1,0:T(8,128)(2,1)} %copy-done.11, bf16[768,256]{1,0:T(8,128)(2,1)} %wq.1, bf16[768,128]{1,0:T(8,128)(2,1)} %nq.1, bf16[4,256]{1,0:T(4,128)(2,1)} %kwq.1, bf16[4,128]{1,0:T(4,128)(2,1)} %knq.1, bf16[768,384]{1,0:T(8,128)(2,1)} %get-tuple-element.50.kk, ...), custom_call_target="tpu_custom_call" | custom-call | flops 8000000000 | bytes 6000000 | tf_op jit(solution)/shard_map/pallas_call | solution.py:483
  44.4 1.6 all-to-all-done
  46.5 12.6 %collective-permute-start.1 = (bf16[64,256]{1,0:T(8,128)(2,1)S(1)}, bf16[64,256]{1,0:T(8,128)(2,1)S(1)}, u32[]{:S(2)}, u32[]{:S(2)}) collective-permute-start(bf16[64,256]{1,0:T(8,128)(2,1)S(1)} %get-tuple-element.62), channel_id=1, source_target_pairs={{0,32},{4,36},{8,40},{12,44},{16,48},{20,52},{24,56},{28,60},{32,6... | collective-permute-start | bytes 98312 | tf_op jit(solution)/shard_map/ppermute | solution.py:515
  59.1 13.7 %collective-permute-start.2 = (bf16[64,256]{1,0:T(8,128)(2,1)S(1)}, bf16[64,256]{1,0:T(8,128)(2,1)S(1)}, u32[]{:S(2)}, u32[]{:S(2)}) collective-permute-start(bf16[64,256]{1,0:T(8,128)(2,1)S(1)} %get-tuple-element.62), channel_id=1, source_target_pairs={{0,64},{4,68},{8,72},{12,76},{16,80},{20,84},{24,88},{28,92},{32,9... | collective-permute-start | bytes 98312 | tf_op jit(solution)/shard_map/ppermute | solution.py:515
  74.4 3.6 %collective-permute-done.3.refs_2_ = bf16[64,256]{1,0:T(8,128)(2,1)S(1)} collective-permute-done((bf16[64,256]{1,0:T(8,128)(2,1)S(1)}, bf16[64,256]{1,0:T(8,128)(2,1)S(1)}, u32[]{:S(2)}, u32[]{:S(2)}) %collective-permute-start.3) | collective-permute-done | bytes 32800 | tf_op jit(solution)/shard_map/ppermute | solution.py:515
  78.1 1.3 shard_map.266
  79.4 3.6 %all-to-all-start.1 = ((bf16[8,64,256]{2,1,0:T(8,128)(2,1)}), bf16[8,64,256]{2,1,0:T(8,128)(2,1)S(1)}, u32[]{:S(2)}, u32[]{:S(2)}) async-start(bf16[8,64,256]{2,1,0:T(8,128)(2,1)} %bitcast.7), calls=%async_computation.1 | async-start | bytes 524288 | tf_op jit(solution)/shard_map/all_to_all | solution.py:481
  83.1 9.5 %all-to-all-done.1 = bf16[8,64,256]{2,1,0:T(8,128)(2,1)S(1)} async-done(((bf16[8,64,256]{2,1,0:T(8,128)(2,1)}), bf16[8,64,256]{2,1,0:T(8,128)(2,1)S(1)}, u32[]{:S(2)}, u32[]{:S(2)}) %all-to-all-start.1) | async-done | bytes 262176 | tf_op jit(solution)/shard_map/all_to_all | solution.py:481
  92.8 5.8 %shard_map.270 = (bf16[96,2048]{1,0:T(8,128)(2,1)S(1)}, bf16[96,2048]{1,0:T(8,128)(2,1)S(1)}) custom-call(s32[1]{0:T(128)} %bitcast._, f32[768,1024]{1,0:T(8,128)} %get-tuple-element.55.refs_0_.refs_4_, bf16[768,384]{1,0:T(8,128)(2,1)} %get-tuple-element.56.refs_1_.refs_5_, f32[768,16]{1,0:T(8,128)} %get-tuple-element.57.refs_2_.refs_6_, ...), custom_call_target="tpu_custom_call" | custom-call | flops 805306368 | bytes 6000000 | tf_op jit(solution)/shard_map/pallas_call | solution.py:540
  99.0 1.8 collective-permute-start.8
  100.8 8.4 %shard_map.269 = (bf16[96,2048]{1,0:T(8,128)(2,1)S(1)}, bf16[96,2048]{1,0:T(8,128)(2,1)S(1)}, bf16[96,2048]{1,0:T(8,128)(2,1)S(1)}, bf16[96,2048]{1,0:T(8,128)(2,1)S(1)}) custom-call(s32[1]{0:T(128)} %bitcast._, f32[768,1024]{1,0:T(8,128)} %get-tuple-element.55.refs_0_.refs_4_, bf16[768,384]{1,0:T(8,128)(2,1)} %get-tuple-element.56.refs_1_.refs_5_, ...), custom_call_target="tpu_custom_call" | custom-call | flops 1610612736 | bytes 6000000 | tf_op jit(solution)/shard_map/pallas_call | solution.py:540
  110.1 2.7 %collective-permute-start.5 = (bf16[96,2048]{1,0:T(8,128)(2,1)S(1)}, bf16[96,2048]{1,0:T(8,128)(2,1)S(1)}, u32[]{:S(2)}, u32[]{:S(2)}) collective-permute-start(bf16[96,2048]{1,0:T(8,128)(2,1)S(1)} %shard_map.271), channel_id=1, source_target_pairs={{0,1},{1,2},{2,3},{3,0},{4,5},{5,6},{6,7},{7,4},{8,9},{9,10},{10,1... | collective-permute-start | bytes 1179656 | tf_op jit(solution)/shard_map/ppermute | solution.py:345
  113.2 1.8 collective-permute-start.9
  115.0 5.8 %shard_map.268 = (bf16[96,2048]{1,0:T(8,128)(2,1)S(1)}, bf16[96,2048]{1,0:T(8,128)(2,1)S(1)}) custom-call(s32[1]{0:T(128)} %bitcast._, f32[768,1024]{1,0:T(8,128)} %get-tuple-element.55.refs_0_.refs_4_, bf16[768,384]{1,0:T(8,128)(2,1)} %get-tuple-element.56.refs_1_.refs_5_, f32[768,16]{1,0:T(8,128)} %get-tuple-element.57.refs_2_.refs_6_, ...), custom_call_target="tpu_custom_call" | custom-call | flops 805306368 | bytes 6000000 | tf_op jit(solution)/shard_map/pallas_call | solution.py:540
  120.8 1.7 collective-permute-done.6.two
  122.9 3.6 %collective-permute-start.10 = (bf16[96,2048]{1,0:T(8,128)(2,1)S(1)}, bf16[96,2048]{1,0:T(8,128)(2,1)S(1)}, u32[]{:S(2)}, u32[]{:S(2)}) collective-permute-start(bf16[96,2048]{1,0:T(8,128)(2,1)S(1)} %get-tuple-element.72.refs_0_), channel_id=1, source_target_pairs={{0,1},{1,2},{2,3},{3,0},{4,5},{5,6},{6,7},{7,4},{8,9},{9,10},{10,1... | collective-permute-start | bytes 1179656 | tf_op jit(solution)/shard_map/ppermute | solution.py:345
  126.4 4.2 %collective-permute-done.7.one = bf16[96,2048]{1,0:T(8,128)(2,1)S(1)} collective-permute-done((bf16[96,2048]{1,0:T(8,128)(2,1)S(1)}, bf16[96,2048]{1,0:T(8,128)(2,1)S(1)}, u32[]{:S(2)}, u32[]{:S(2)}) %collective-permute-start.7) | collective-permute-done | bytes 393248 | tf_op jit(solution)/shard_map/ppermute | solution.py:345
  132.2 4.8 %collective-permute-done.10.refs_0_ = bf16[96,2048]{1,0:T(8,128)(2,1)S(1)} collective-permute-done((bf16[96,2048]{1,0:T(8,128)(2,1)S(1)}, bf16[96,2048]{1,0:T(8,128)(2,1)S(1)}, u32[]{:S(2)}, u32[]{:S(2)}) %collective-permute-start.10) | collective-permute-done | bytes 393248 | tf_op jit(solution)/shard_map/ppermute | solution.py:345
  137.0 3.7 %collective-permute-start.14 = (bf16[96,2048]{1,0:T(8,128)(2,1)S(1)}, bf16[96,2048]{1,0:T(8,128)(2,1)S(1)}, u32[]{:S(2)}, u32[]{:S(2)}) collective-permute-start(bf16[96,2048]{1,0:T(8,128)(2,1)S(1)} %collective-permute-done.10.refs_0_), channel_id=1, source_target_pairs={{0,1},{1,2},{2,3},{3,0},{4,5},{5,6},{6,7},{7,4},{8,9},{9,10},{10,1... | collective-permute-start | bytes 1179656 | tf_op jit(solution)/shard_map/ppermute | solution.py:345
  141.2 3.8 %collective-permute-start.11 = (bf16[96,2048]{1,0:T(8,128)(2,1)S(1)}, bf16[96,2048]{1,0:T(8,128)(2,1)S(1)}, u32[]{:S(2)}, u32[]{:S(2)}) collective-permute-start(bf16[96,2048]{1,0:T(8,128)(2,1)S(1)} %get-tuple-element.77.refs_1_), channel_id=1, source_target_pairs={{0,1},{1,2},{2,3},{3,0},{4,5},{5,6},{6,7},{7,4},{8,9},{9,10},{10,1... | collective-permute-start | bytes 1179656 | tf_op jit(solution)/shard_map/ppermute | solution.py:345
  145.1 5.1 %collective-permute-done.14.refs_0_ = bf16[96,2048]{1,0:T(8,128)(2,1)S(1)} collective-permute-done((bf16[96,2048]{1,0:T(8,128)(2,1)S(1)}, bf16[96,2048]{1,0:T(8,128)(2,1)S(1)}, u32[]{:S(2)}, u32[]{:S(2)}) %collective-permute-start.14) | collective-permute-done | bytes 393248 | tf_op jit(solution)/shard_map/ppermute | solution.py:345
  150.2 4.8 %collective-permute-done.15.refs_1_ = bf16[96,2048]{1,0:T(8,128)(2,1)S(1)} collective-permute-done((bf16[96,2048]{1,0:T(8,128)(2,1)S(1)}, bf16[96,2048]{1,0:T(8,128)(2,1)S(1)}, u32[]{:S(2)}, u32[]{:S(2)}) %collective-permute-start.15) | collective-permute-done | bytes 393248 | tf_op jit(solution)/shard_map/ppermute | solution.py:345
  155.9 6.1 %shard_map.277 = (bf16[96,2048]{1,0:T(8,128)(2,1)S(1)}, bf16[96,2048]{1,0:T(8,128)(2,1)S(1)}) custom-call(bf16[96,2048]{1,0:T(8,128)(2,1)S(1)} %collective-permute-done.14.refs_0_, bf16[96,2048]{1,0:T(8,128)(2,1)S(1)} %collective-permute-done.15.refs_1_, bf16[2048,2304]{1,0:T(8,128)(2,1)} %all-gather.2.cloned.1.call-done.refs_2_.refs_3_.refs_4_.refs_5_.refs_6_, ...), custom_call_target="tpu_custom_call" | custom-call | flops 1811939328 | bytes 9437184 | tf_op jit(solution)/shard_map/pallas_call | solution.py:355
  164.2 7.4 %shard_map.276 = (bf16[96,2048]{1,0:T(8,128)(2,1)S(1)}, bf16[96,2048]{1,0:T(8,128)(2,1)S(1)}, bf16[96,2048]{1,0:T(8,128)(2,1)S(1)}, bf16[96,2048]{1,0:T(8,128)(2,1)S(1)}) custom-call(bf16[96,2048]{1,0:T(8,128)(2,1)S(1)} %collective-permute-done.10.refs_0_, bf16[96,2048]{1,0:T(8,128)(2,1)S(1)} %collective-permute-done.11.refs_1_, ...), custom_call_target="tpu_custom_call" | custom-call | flops 3623878656 | bytes 9437184 | tf_op jit(solution)/shard_map/pallas_call | solution.py:355
  172.8 2.4 %collective-permute-start.19 = (bf16[96,2048]{1,0:T(8,128)(2,1)S(1)}, bf16[96,2048]{1,0:T(8,128)(2,1)S(1)}, u32[]{:S(2)}, u32[]{:S(2)}) collective-permute-start(bf16[96,2048]{1,0:T(8,128)(2,1)S(1)} %get-tuple-element.85), channel_id=1, source_target_pairs={{0,1},{1,2},{2,3},{3,0},{4,5},{5,6},{6,7},{7,4},{8,9},{9,10},{10,1... | collective-permute-start | bytes 1179656 | tf_op jit(solution)/shard_map/ppermute | solution.py:345
  177.7 6.2 %shard_map.275 = (bf16[96,2048]{1,0:T(8,128)(2,1)S(1)}, bf16[96,2048]{1,0:T(8,128)(2,1)S(1)}) custom-call(bf16[96,2048]{1,0:T(8,128)(2,1)S(1)} %get-tuple-element.72.refs_0_, bf16[96,2048]{1,0:T(8,128)(2,1)S(1)} %get-tuple-element.77.refs_1_, bf16[2048,2304]{1,0:T(8,128)(2,1)} %all-gather.2.cloned.1.call-done.refs_2_.refs_3_.refs_4_.refs_5_.refs_6_, ...), custom_call_target="tpu_custom_call" | custom-call | flops 1811939328 | bytes 9437184 | tf_op jit(solution)/shard_map/pallas_call | solution.py:355
  183.8 1.3 collective-permute-done.18.t2
  185.2 6.4 %collective-permute-done.17.t1 = bf16[96,2048]{1,0:T(8,128)(2,1)S(1)} collective-permute-done((bf16[96,2048]{1,0:T(8,128)(2,1)S(1)}, bf16[96,2048]{1,0:T(8,128)(2,1)S(1)}, u32[]{:S(2)}, u32[]{:S(2)}) %collective-permute-start.17) | collective-permute-done | bytes 393248 | tf_op jit(solution)/shard_map/ppermute | solution.py:345
  (64 shorter events, 17.0 us)
Async XLA Ops:
  8.4 2.9 %collective-permute-start = (bf16[8,1792]{1,0:T(8,128)(2,1)}, bf16[8,1792]{1,0:T(8,128)(2,1)S(1)}, u32[]{:S(2)}, u32[]{:S(2)}) collective-permute-start(bf16[8,1792]{1,0:T(8,128)(2,1)} %get-tuple-element.47), channel_id=1, source_target_pairs={{0,4},{4,8},{8,12},{12,16},{16,20},{20,24},{24,28},{28,32},{32,36}... | collective-permute-start | bytes 86024 | tf_op jit(solution)/shard_map/ppermute | solution.py:443
  23.8 22.2 %all-to-all-start = ((bf16[8,64,256]{2,1,0:T(8,128)(2,1)}), bf16[8,64,256]{2,1,0:T(8,128)(2,1)S(1)}, u32[]{:S(2)}, u32[]{:S(2)}) async-start(bf16[8,64,256]{2,1,0:T(8,128)(2,1)} %bitcast.11), calls=%async_computation | async-start | bytes 524288 | tf_op jit(solution)/shard_map/all_to_all | solution.py:481
  36.2 119.7 %all-gather.2.cloned.1.call-start = ((), (), s32[]{:S(2)}) async-start(), calls=%async_computation.2 | async-start | bytes 9732096 | tf_op jit(solution)/shard_map/all_gather | solution.py:519
  36.3 9.6 %copy-start.4 = (bf16[16,1024]{1,0:T(8,128)(2,1)S(1)}, bf16[16,1024]{1,0:T(8,128)(2,1)}, u32[]{:S(2)}) copy-start(bf16[16,1024]{1,0:T(8,128)(2,1)} %constant.28.clone.table.refs_7_.refs_11_) | copy-start | bytes 98308
  36.3 9.6 %copy-start.6 = (bf16[256,16]{1,0:T(8,128)(2,1)S(1)}, bf16[256,16]{1,0:T(8,128)(2,1)}, u32[]{:S(2)}) copy-start(bf16[256,16]{1,0:T(8,128)(2,1)} %constant.31.clone.unplace) | copy-start | bytes 24580
  36.3 9.6 %copy-start.7 = (bf16[16,512]{1,0:T(8,128)(2,1)S(1)}, bf16[16,512]{1,0:T(8,128)(2,1)}, u32[]{:S(2)}) copy-start(bf16[16,512]{1,0:T(8,128)(2,1)} %constant.30.clone.place) | copy-start | bytes 49156
  36.3 9.6 %copy-start.8 = (bf16[8,512]{1,0:T(8,128)(2,1)S(1)}, bf16[8,512]{1,0:T(8,128)(2,1)}, u32[]{:S(2)}) copy-start(bf16[8,512]{1,0:T(8,128)(2,1)} %constant.34.clone.gather) | copy-start | bytes 24580
  46.5 27.6 %collective-permute-start.1 = (bf16[64,256]{1,0:T(8,128)(2,1)S(1)}, bf16[64,256]{1,0:T(8,128)(2,1)S(1)}, u32[]{:S(2)}, u32[]{:S(2)}) collective-permute-start(bf16[64,256]{1,0:T(8,128)(2,1)S(1)} %get-tuple-element.62), channel_id=1, source_target_pairs={{0,32},{4,36},{8,40},{12,44},{16,48},{20,52},{24,56},{28,60},{32,6... | collective-permute-start | bytes 98312 | tf_op jit(solution)/shard_map/ppermute | solution.py:515
  59.1 15.3 %collective-permute-start.2 = (bf16[64,256]{1,0:T(8,128)(2,1)S(1)}, bf16[64,256]{1,0:T(8,128)(2,1)S(1)}, u32[]{:S(2)}, u32[]{:S(2)}) collective-permute-start(bf16[64,256]{1,0:T(8,128)(2,1)S(1)} %get-tuple-element.62), channel_id=1, source_target_pairs={{0,64},{4,68},{8,72},{12,76},{16,80},{20,84},{24,88},{28,92},{32,9... | collective-permute-start | bytes 98312 | tf_op jit(solution)/shard_map/ppermute | solution.py:515
  72.8 5.2 %collective-permute-start.3 = (bf16[64,256]{1,0:T(8,128)(2,1)S(1)}, bf16[64,256]{1,0:T(8,128)(2,1)S(1)}, u32[]{:S(2)}, u32[]{:S(2)}) collective-permute-start(bf16[64,256]{1,0:T(8,128)(2,1)S(1)} %get-tuple-element.62), channel_id=1, source_target_pairs={{0,96},{4,100},{8,104},{12,108},{16,112},{20,116},{24,120},{28,124... | collective-permute-start | bytes 98312 | tf_op jit(solution)/shard_map/ppermute | solution.py:515
  78.1 14.5 %copy-start.1 = (bf16[384,512]{1,0:T(8,128)(2,1)S(1)}, bf16[384,512]{1,0:T(8,128)(2,1)}, u32[]{:S(2)}) copy-start(bf16[384,512]{1,0:T(8,128)(2,1)} %constant.33.clone.unpick) | copy-start | bytes 1179652
  78.1 14.7 %copy-start = (bf16[1024,16]{1,0:T(8,128)(2,1)S(1)}, bf16[1024,16]{1,0:T(8,128)(2,1)}, u32[]{:S(2)}) copy-start(bf16[1024,16]{1,0:T(8,128)(2,1)} %constant.29.clone.refs_8_.refs_12_) | copy-start | bytes 98308
  79.4 13.1 %all-to-all-start.1 = ((bf16[8,64,256]{2,1,0:T(8,128)(2,1)}), bf16[8,64,256]{2,1,0:T(8,128)(2,1)S(1)}, u32[]{:S(2)}, u32[]{:S(2)}) async-start(bf16[8,64,256]{2,1,0:T(8,128)(2,1)} %bitcast.7), calls=%async_computation.1 | async-start | bytes 524288 | tf_op jit(solution)/shard_map/all_to_all | solution.py:481
  98.7 11.3 %collective-permute-start.4 = (bf16[96,2048]{1,0:T(8,128)(2,1)S(1)}, bf16[96,2048]{1,0:T(8,128)(2,1)S(1)}, u32[]{:S(2)}, u32[]{:S(2)}) collective-permute-start(bf16[96,2048]{1,0:T(8,128)(2,1)S(1)} %get-tuple-element.69), channel_id=1, source_target_pairs={{0,1},{1,2},{2,3},{3,0},{4,5},{5,6},{6,7},{7,4},{8,9},{9,10},{10,1... | collective-permute-start | bytes 1179656 | tf_op jit(solution)/shard_map/ppermute | solution.py:345
  99.0 14.0 %collective-permute-start.8 = (bf16[96,2048]{1,0:T(8,128)(2,1)S(1)}, bf16[96,2048]{1,0:T(8,128)(2,1)S(1)}, u32[]{:S(2)}, u32[]{:S(2)}) collective-permute-start(bf16[96,2048]{1,0:T(8,128)(2,1)S(1)} %get-tuple-element.76), channel_id=1, source_target_pairs={{0,3},{1,0},{2,1},{3,2},{4,7},{5,4},{6,5},{7,6},{8,11},{9,8},{10,9... | collective-permute-start | bytes 1179656 | tf_op jit(solution)/shard_map/ppermute | solution.py:345
  109.2 13.3 %collective-permute-start.6 = (bf16[96,2048]{1,0:T(8,128)(2,1)S(1)}, bf16[96,2048]{1,0:T(8,128)(2,1)S(1)}, u32[]{:S(2)}, u32[]{:S(2)}) collective-permute-start(bf16[96,2048]{1,0:T(8,128)(2,1)S(1)} %get-tuple-element.70), channel_id=1, source_target_pairs={{0,3},{1,0},{2,1},{3,2},{4,7},{5,4},{6,5},{7,6},{8,11},{9,8},{10,9... | collective-permute-start | bytes 1179656 | tf_op jit(solution)/shard_map/ppermute | solution.py:345
  110.1 12.4 %collective-permute-start.5 = (bf16[96,2048]{1,0:T(8,128)(2,1)S(1)}, bf16[96,2048]{1,0:T(8,128)(2,1)S(1)}, u32[]{:S(2)}, u32[]{:S(2)}) collective-permute-start(bf16[96,2048]{1,0:T(8,128)(2,1)S(1)} %shard_map.271), channel_id=1, source_target_pairs={{0,1},{1,2},{2,3},{3,0},{4,5},{5,6},{6,7},{7,4},{8,9},{9,10},{10,1... | collective-permute-start | bytes 1179656 | tf_op jit(solution)/shard_map/ppermute | solution.py:345
  112.7 17.9 %collective-permute-start.7 = (bf16[96,2048]{1,0:T(8,128)(2,1)S(1)}, bf16[96,2048]{1,0:T(8,128)(2,1)S(1)}, u32[]{:S(2)}, u32[]{:S(2)}) collective-permute-start(bf16[96,2048]{1,0:T(8,128)(2,1)S(1)} %get-tuple-element.74), channel_id=1, source_target_pairs={{0,1},{1,2},{2,3},{3,0},{4,5},{5,6},{6,7},{7,4},{8,9},{9,10},{10,1... | collective-permute-start | bytes 1179656 | tf_op jit(solution)/shard_map/ppermute | solution.py:345
  113.2 17.5 %collective-permute-start.9 = (bf16[96,2048]{1,0:T(8,128)(2,1)S(1)}, bf16[96,2048]{1,0:T(8,128)(2,1)S(1)}, u32[]{:S(2)}, u32[]{:S(2)}) collective-permute-start(bf16[96,2048]{1,0:T(8,128)(2,1)S(1)} %shard_map.273), channel_id=1, source_target_pairs={{0,3},{1,0},{2,1},{3,2},{4,7},{5,4},{6,5},{7,6},{8,11},{9,8},{10,9... | collective-permute-start | bytes 1179656 | tf_op jit(solution)/shard_map/ppermute | solution.py:345
  122.9 14.1 %collective-permute-start.10 = (bf16[96,2048]{1,0:T(8,128)(2,1)S(1)}, bf16[96,2048]{1,0:T(8,128)(2,1)S(1)}, u32[]{:S(2)}, u32[]{:S(2)}) collective-permute-start(bf16[96,2048]{1,0:T(8,128)(2,1)S(1)} %get-tuple-element.72.refs_0_), channel_id=1, source_target_pairs={{0,1},{1,2},{2,3},{3,0},{4,5},{5,6},{6,7},{7,4},{8,9},{9,10},{10,1... | collective-permute-start | bytes 1179656 | tf_op jit(solution)/shard_map/ppermute | solution.py:345
  131.8 9.4 %collective-permute-start.13 = (bf16[96,2048]{1,0:T(8,128)(2,1)S(1)}, bf16[96,2048]{1,0:T(8,128)(2,1)S(1)}, u32[]{:S(2)}, u32[]{:S(2)}) collective-permute-start(bf16[96,2048]{1,0:T(8,128)(2,1)S(1)} %get-tuple-element.77.refs_1_), channel_id=1, source_target_pairs={{0,3},{1,0},{2,1},{3,2},{4,7},{5,4},{6,5},{7,6},{8,11},{9,8},{10,9... | collective-permute-start | bytes 1179656 | tf_op jit(solution)/shard_map/ppermute | solution.py:345
  137.0 13.2 %collective-permute-start.14 = (bf16[96,2048]{1,0:T(8,128)(2,1)S(1)}, bf16[96,2048]{1,0:T(8,128)(2,1)S(1)}, u32[]{:S(2)}, u32[]{:S(2)}) collective-permute-start(bf16[96,2048]{1,0:T(8,128)(2,1)S(1)} %collective-permute-done.10.refs_0_), channel_id=1, source_target_pairs={{0,1},{1,2},{2,3},{3,0},{4,5},{5,6},{6,7},{7,4},{8,9},{9,10},{10,1... | collective-permute-start | bytes 1179656 | tf_op jit(solution)/shard_map/ppermute | solution.py:345
  141.2 13.8 %collective-permute-start.15 = (bf16[96,2048]{1,0:T(8,128)(2,1)S(1)}, bf16[96,2048]{1,0:T(8,128)(2,1)S(1)}, u32[]{:S(2)}, u32[]{:S(2)}) collective-permute-start(bf16[96,2048]{1,0:T(8,128)(2,1)S(1)} %collective-permute-done.13.refs_3_), channel_id=1, source_target_pairs={{0,3},{1,0},{2,1},{3,2},{4,7},{5,4},{6,5},{7,6},{8,11},{9,8},{10,9... | collective-permute-start | bytes 1179656 | tf_op jit(solution)/shard_map/ppermute | solution.py:345
  141.2 23.0 %collective-permute-start.11 = (bf16[96,2048]{1,0:T(8,128)(2,1)S(1)}, bf16[96,2048]{1,0:T(8,128)(2,1)S(1)}, u32[]{:S(2)}, u32[]{:S(2)}) collective-permute-start(bf16[96,2048]{1,0:T(8,128)(2,1)S(1)} %get-tuple-element.77.refs_1_), channel_id=1, source_target_pairs={{0,1},{1,2},{2,3},{3,0},{4,5},{5,6},{6,7},{7,4},{8,9},{9,10},{10,1... | collective-permute-start | bytes 1179656 | tf_op jit(solution)/shard_map/ppermute | solution.py:345
  145.1 19.1 %collective-permute-start.12 = (bf16[96,2048]{1,0:T(8,128)(2,1)S(1)}, bf16[96,2048]{1,0:T(8,128)(2,1)S(1)}, u32[]{:S(2)}, u32[]{:S(2)}) collective-permute-start(bf16[96,2048]{1,0:T(8,128)(2,1)S(1)} %get-tuple-element.72.refs_0_), channel_id=1, source_target_pairs={{0,3},{1,0},{2,1},{3,2},{4,7},{5,4},{6,5},{7,6},{8,11},{9,8},{10,9... | collective-permute-start | bytes 1179656 | tf_op jit(solution)/shard_map/ppermute | solution.py:345
  162.1 13.1 %collective-permute-start.16 = (bf16[96,2048]{1,0:T(8,128)(2,1)S(1)}, bf16[96,2048]{1,0:T(8,128)(2,1)S(1)}, u32[]{:S(2)}, u32[]{:S(2)}) collective-permute-start(bf16[96,2048]{1,0:T(8,128)(2,1)S(1)} %get-tuple-element.81), channel_id=1, source_target_pairs={{0,1},{1,2},{2,3},{3,0},{4,5},{5,6},{6,7},{7,4},{8,9},{9,10},{10,1... | collective-permute-start | bytes 1179656 | tf_op jit(solution)/shard_map/ppermute | solution.py:345
  163.2 13.2 %collective-permute-start.20 = (bf16[96,2048]{1,0:T(8,128)(2,1)S(1)}, bf16[96,2048]{1,0:T(8,128)(2,1)S(1)}, u32[]{:S(2)}, u32[]{:S(2)}) collective-permute-start(bf16[96,2048]{1,0:T(8,128)(2,1)S(1)} %get-tuple-element.87), channel_id=1, source_target_pairs={{0,3},{1,0},{2,1},{3,2},{4,7},{5,4},{6,5},{7,6},{8,11},{9,8},{10,9... | collective-permute-start | bytes 1179656 | tf_op jit(solution)/shard_map/ppermute | solution.py:345
  171.6 13.5 %collective-permute-start.18 = (bf16[96,2048]{1,0:T(8,128)(2,1)S(1)}, bf16[96,2048]{1,0:T(8,128)(2,1)S(1)}, u32[]{:S(2)}, u32[]{:S(2)}) collective-permute-start(bf16[96,2048]{1,0:T(8,128)(2,1)S(1)} %get-tuple-element.82), channel_id=1, source_target_pairs={{0,3},{1,0},{2,1},{3,2},{4,7},{5,4},{6,5},{7,6},{8,11},{9,8},{10,9... | collective-permute-start | bytes 1179656 | tf_op jit(solution)/shard_map/ppermute | solution.py:345
  172.8 12.4 %collective-permute-start.19 = (bf16[96,2048]{1,0:T(8,128)(2,1)S(1)}, bf16[96,2048]{1,0:T(8,128)(2,1)S(1)}, u32[]{:S(2)}, u32[]{:S(2)}) collective-permute-start(bf16[96,2048]{1,0:T(8,128)(2,1)S(1)} %get-tuple-element.85), channel_id=1, source_target_pairs={{0,1},{1,2},{2,3},{3,0},{4,5},{5,6},{6,7},{7,4},{8,9},{9,10},{10,1... | collective-permute-start | bytes 1179656 | tf_op jit(solution)/shard_map/ppermute | solution.py:345
  175.3 16.3 %collective-permute-start.17 = (bf16[96,2048]{1,0:T(8,128)(2,1)S(1)}, bf16[96,2048]{1,0:T(8,128)(2,1)S(1)}, u32[]{:S(2)}, u32[]{:S(2)}) collective-permute-start(bf16[96,2048]{1,0:T(8,128)(2,1)S(1)} %shard_map.278), channel_id=1, source_target_pairs={{0,1},{1,2},{2,3},{3,0},{4,5},{5,6},{6,7},{7,4},{8,9},{9,10},{10,1... | collective-permute-start | bytes 1179656 | tf_op jit(solution)/shard_map/ppermute | solution.py:345
  176.5 15.8 %copy-start.3 = (bf16[96,2048]{1,0:T(8,128)(2,1)S(1)}, bf16[96,2048]{1,0:T(8,128)(2,1)}, u32[]{:S(2)}) copy-start(bf16[96,2048]{1,0:T(8,128)(2,1)} %copy-done.2) | copy-start | bytes 1179652
  176.5 15.8 %collective-permute-start.21 = (bf16[96,2048]{1,0:T(8,128)(2,1)S(1)}, bf16[96,2048]{1,0:T(8,128)(2,1)S(1)}, u32[]{:S(2)}, u32[]{:S(2)}) collective-permute-start(bf16[96,2048]{1,0:T(8,128)(2,1)S(1)} %shard_map.279), channel_id=1, source_target_pairs={{0,3},{1,0},{2,1},{3,2},{4,7},{5,4},{6,5},{7,6},{8,11},{9,8},{10,9... | collective-permute-start | bytes 1179656 | tf_op jit(solution)/shard_map/ppermute | solution.py:345
  (5 other events, 18.1 us)
Sparse Core Ops, SparseCore 0:
  78.2 77.6 all-gather.1
where the time goes:
time: 204 us; the launch traced here: 200 us
  starting transfers between devices  72.7 us (36%)
  Pallas kernels  66 us (32%)
  waiting for transfers between devices  46.6 us (23%)
  between operations  13.7 us (7%)
    ppermute x18, waiting for transfers between devices, ring(): lax.ppermute(value, axis, [(i, (i + step) % count) for i in range(count)])  29.7 us
    ppermute x3, starting transfers between devices, on_device(): lax.ppermute(sent, 'sp', [(i, i + near * n) for i in range(sp - near * n)])  27.6 us
    ppermute x18, starting transfers between devices, ring(): lax.ppermute(value, axis, [(i, (i + step) % count) for i in range(count)])  27.2 us
    pallas_call x3, Pallas kernels, project(): pl.pallas_call(functools.partial(project_kernel, groups, count), grid_spe...  20 us
    pallas_call x3, Pallas kernels, feed(): pl.pallas_call(functools.partial(feed_kernel, len(xs)), grid=(tiles,), in...  19.7 us
    all_to_all x2, starting transfers between devices, on_device(): lax.all_to_all(a, 'sp', 0, 0, axis_index_groups=seats, tiled=True)  16.1 us
    pallas_call x1, Pallas kernels, on_device(): pl.pallas_call(functools.partial(states_kernel, groups, chunk), grid=(blo...  11.9 us
    all_to_all x2, waiting for transfers between devices, on_device(): lax.all_to_all(a, 'sp', 0, 0, axis_index_groups=seats, tiled=True)  11 us
  transfers between devices with their start and end apart: 25, of which 15 were waited for; matrix products, arithmetic and copies ran while one was open for 0% of the time, Pallas kernels for 25%

commit v1 on v0

--- a/solution.py
+++ b/solution.py
@@ -16,6 +16,8 @@
 WIDE = 128
 NARROW = 64
 TAPS = 4
+LANES = 128
+STRIP = 32
 EDGE = 8
 EPS = 1e-6
 F32 = jnp.float32
@@ -44,6 +46,11 @@
 
 def dot2(pair, b):
     return dot(pair[0], b) + dot(pair[1], b)
+
+
+def stacked_columns(x):
+    hi = x.astype(BF16).astype(F32)
+    return jnp.concatenate([hi, x - hi], axis=0).T.astype(BF16)
 
 
 def silu(x):
@@ -62,24 +69,34 @@
     return out, row
 
 
-def conv_cols(buf, cols, ker):
+def fill(buf, rows, x):
+    for n in range(x.shape[1] // LANES):
+        buf[n, rows, :] = x[:, n * LANES : (n + 1) * LANES].astype(F32)
+
+
+def conv_plane(buf, plane, ker, row):
     k = ker.astype(F32)
-    first = EDGE - TAPS + 1
-    total = buf[first : first + BT, cols] * k[0:1]
+    first = row + EDGE - TAPS + 1
+    total = buf[plane, first : first + STRIP, :] * k[0:1]
     for tap in range(1, TAPS):
-        total += buf[first + tap : first + tap + BT, cols] * k[tap : tap + 1]
-    return silu(total)
-
-
-def edge_kernel(*refs):
-    ins, (edge, both) = refs[:-2], refs[-2:]
+        total += buf[plane, first + tap : first + tap + STRIP, :] * k[tap : tap + 1]
+    return silu(total).astype(BF16)
+
+
+def conv_all(buf, kernels, out):
+    plane = 0
+    for ker in kernels:
+        for c in range(0, ker.shape[1], LANES):
+            cols = slice(plane * LANES, (plane + 1) * LANES)
+            for row in range(0, BT, STRIP):
+                out[row : row + STRIP, cols] = conv_plane(buf, plane, ker[:, c : c + LANES], row)
+            plane += 1
+
+
+def join_kernel(*refs):
     at = 0
-    for part in ins[:-3]:
-        edge[:, at : at + part.shape[1]] = part[...]
-        at += part.shape[1]
-    at = 0
-    for part in ins[-3:]:
-        both[:, at : at + part.shape[1]] = part[...]
+    for part in refs[:-1]:
+        refs[-1][:, at : at + part.shape[1]] = part[...]
         at += part.shape[1]
 
 
@@ -93,14 +110,15 @@
 
     @pl.when(i == 0)
     def _():
-        bufv[0:EDGE, :] = rim[:, 0:inner].astype(F32)
-        bufk[0:EDGE, :] = rim[:, inner : inner + wcols + ncols].astype(F32)
+        fill(bufv, slice(0, EDGE), rim[:, 0:inner])
+        fill(bufk, slice(0, EDGE), rim[:, inner : inner + wcols + ncols])
         state[...] = jnp.zeros_like(state)
         before[...] = jnp.zeros_like(before)
 
-    bufv[EDGE:, :] = value[...].astype(F32)
-    bufk[EDGE:, 0:wcols] = wk[...].astype(F32)
-    bufk[EDGE:, wcols:] = nk[...].astype(F32)
+    body = slice(EDGE, EDGE + BT)
+    fill(bufv, body, value)
+    fill(bufk, body, wk)
+    fill(bufk.at[wcols // LANES :], body, nk)
 
     heads = step.shape[0]
     diagonal = lax.broadcasted_iota(jnp.int32, (heads, heads), 0) == lax.broadcasted_iota(
@@ -117,34 +135,34 @@
     a2, a3 = halves(a - a1.astype(F32))
     r = dot(a1, upto) + dot(a2, upto) + dot(a3, upto)
     mid, end = r[:, BT // 2 - 1 : BT // 2], r[:, BT - 1 : BT]
-    er[...] = jnp.exp(r - mid).T
-    eR[...] = jnp.exp(r + before[...]).T
+    er[...] = stacked_columns(jnp.exp(r - mid))
+    eR[...] = stacked_columns(jnp.exp(r + before[...]))
     before[...] = before[...] + end
-    inward = halves((jnp.exp(mid - r) * dt).T)
+    inward = stacked_columns(jnp.exp(mid - r) * dt)
     lane = lax.broadcasted_iota(jnp.int32, r.shape, 1)
     scales = jnp.exp(jnp.where(lane == 0, mid, jnp.where(lane == 1, end, end - mid)))
-    scales = halves(scales.T[0:8])
-
-    for c in range(0, wcols, 128):
-        cols = slice(c, c + 128)
-        kk[:, cols] = conv_cols(bufk, cols, kwk[:, cols]).astype(BF16)
-    for c in range(0, ncols, 128):
-        cols = slice(wcols + c, wcols + c + 128)
-        kk[:, cols] = conv_cols(bufk, cols, knk[:, c : c + 128]).astype(BF16)
+    scales = stacked_columns(scales)[0:16]
+
+    conv_all(bufk, (kwk, knk), kk)
     for g, (row, size, key) in enumerate(info):
         cols = slice(g * GW, (g + 1) * GW)
         tab = table[:, cols]
-        f = dot2(inward, tab)
-        s = dot2(scales, tab)
-        u = conv_cols(bufv, cols, kv[:, cols]).astype(BF16).astype(F32)
-        scaled = (u * f).astype(BF16)
-        up[:, cols] = scaled
+        f = dot(inward, tab)
+        s = dot(scales, tab)
+        for n in range(GW // LANES):
+            plane = g * (GW // LANES) + n
+            part = slice(plane * LANES, (plane + 1) * LANES)
+            for at in range(0, BT, STRIP):
+                strip = slice(at, at + STRIP)
+                u = conv_plane(bufv, plane, kv[:, part], at).astype(F32)
+                up[strip, part] = (u * f[strip, n * LANES : (n + 1) * LANES]).astype(BF16)
+        scaled = up[:, cols]
         added = dot_tn(kk[:, key : key + size], scaled)
         old = state[row : row + size, :]
         hs[0, row : row + size, :] = (old * s[0:1]).astype(BF16)
         state[row : row + size, :] = old * s[1:2] + added * s[2:3]
-    bufv[0:EDGE, :] = bufv[BT:, :]
-    bufk[0:EDGE, :] = bufk[BT:, :]
+    bufv[:, 0:EDGE, :] = bufv[:, BT:, :]
+    bufk[:, 0:EDGE, :] = bufk[:, BT:, :]
 
     @pl.when(i == pl.num_programs(0) - 1)
     def _():
@@ -163,18 +181,14 @@
 
     @pl.when(i == 0)
     def _():
-        bufq[0:EDGE, :] = rim[:, rim.shape[1] - wcols - ncols :].astype(F32)
-
-    bufq[EDGE:, 0:wcols] = wq[...].astype(F32)
-    bufq[EDGE:, wcols:] = nq[...].astype(F32)
-    for c in range(0, wcols, 128):
-        cols = slice(c, c + 128)
-        qq[:, cols] = conv_cols(bufq, cols, kwq[:, cols]).astype(BF16)
-    for c in range(0, ncols, 128):
-        cols = slice(wcols + c, wcols + c + 128)
-        qq[:, cols] = conv_cols(bufq, cols, knq[:, c : c + 128]).astype(BF16)
-    bufq[0:EDGE, :] = bufq[BT:, :]
-    outward = halves(er[...])
+        fill(bufq, slice(0, EDGE), rim[:, rim.shape[1] - wcols - ncols :])
+
+    body = slice(EDGE, EDGE + BT)
+    fill(bufq, body, wq)
+    fill(bufq.at[wcols // LANES :], body, nq)
+    conv_all(bufq, (kwq, knq), qq)
+    bufq[:, 0:EDGE, :] = bufq[:, BT:, :]
+    outward = er[...]
     t = lax.broadcasted_iota(jnp.int32, (BT, BT), 0)
     s = lax.broadcasted_iota(jnp.int32, (BT, BT), 1)
     for g, (row, size, key) in enumerate(info):
@@ -182,13 +196,14 @@
         q, k = qq[:, key : key + size], kk[:, key : key + size]
         weights = jnp.where(s <= t, dot_nt(q, k), 0.0).astype(BF16)
         y = dot(weights, up[:, cols]) + dot(q, hs[0, row : row + size, :])
-        yl[:, cols] = y * dot2(outward, table[:, cols])
+        yl[:, cols] = y * dot(outward, table[:, cols])
 
 
 def row_fades(groups, used, padded, place, sums, table):
     info, _ = group_rows(groups)
     factor = halves(jnp.exp(sums))
-    fades = [dot2(factor, table[:, g * GW : (g + 1) * GW]) for g in range(groups)]
+    heads = table.shape[0] // 2
+    fades = [dot2(factor, table[:heads, g * GW : (g + 1) * GW]) for g in range(groups)]
     row = lax.broadcasted_iota(jnp.int32, (padded, GW), 0) + place * used
     masks = [row >= info[g][0] for g in range(1, groups)]
 
@@ -248,19 +263,19 @@
     def _():
         for n in range(count):
             yl, qq, eR, gate = ins[4 * n : 4 * n + 4]
-            reach = halves(eR[...])
-            squares = jnp.zeros((share, table.shape[0]), F32)
+            reach = eR[...]
+            squares = jnp.zeros((share, table.shape[0] // 2), F32)
             for g, (row, size, key) in enumerate(info):
                 cols = slice(g * GW, (g + 1) * GW)
                 outer = dot(qq[:, key : key + size], hin[row : row + size, :])
-                y = yl[:, cols] + outer * dot2(reach, table[:, cols])
+                y = yl[:, cols] + outer * dot(reach, table[:, cols])
                 gated = y * silu(gate[:, cols].astype(F32))
                 held[:, cols] = gated
                 squares += dot2(halves(gated * gated), table_t[cols, :])
             scale = halves(lax.rsqrt(squares * (1.0 / CH) + EPS))
             for g in range(groups):
                 cols = slice(g * GW, (g + 1) * GW)
-                unit = held[:, cols] * dot2(scale, table[:, cols]) * gain[:, cols].astype(F32)
+                unit = held[:, cols] * dot2(scale, table[: table.shape[0] // 2, cols]) * gain[:, cols].astype(F32)
                 normed[n * share : (n + 1) * share, cols] = unit.astype(BF16)
 
     p = dot(normed[...], matrix[...]).astype(BF16)
@@ -401,7 +416,8 @@
 
     struct = jax.ShapeDtypeStruct
     table_np = (np.arange(heads)[:, None] == np.arange(inner)[None] // CH).astype(np.float32)
-    table, table_t = jnp.asarray(table_np, BF16), jnp.asarray(table_np.T, BF16)
+    table = jnp.asarray(np.concatenate([table_np, table_np]), BF16)
+    table_t = jnp.asarray(table_np.T, BF16)
     place_np = np.zeros((heads, 2 * GW), np.float32)
     place_np[np.arange(heads), np.arange(heads)] = 1
     place_np[np.arange(heads), GW + heads + np.arange(heads)] = 1
@@ -420,31 +436,30 @@
     rowed = (
         value_projected, wide_key_rows, narrow_key_rows, wide_query_rows, narrow_query_rows
     )
-    span = sum(a.shape[1] for a in rowed)
+
+    def joined(arrays, specs):
+        shape = (specs[0].block_shape[0], sum(a.shape[1] for a in arrays))
+        return pl.pallas_call(
+            join_kernel,
+            grid=(1,),
+            in_specs=specs,
+            out_specs=pl.BlockSpec(shape, lambda i: (0, 0)),
+            out_shape=struct(shape, BF16),
+            compiler_params=params(),
+            cost_estimate=cost(1e6, 1e6),
+        )(*arrays)
+
+    ends = [pl.BlockSpec((EDGE, a.shape[1]), lambda i: (length // EDGE - 1, 0)) for a in rowed]
+    edge = joined(rowed, ends)
+    rim = lax.ppermute(edge, "sp", [(i, i + 1) for i in range(sp - 1)])
+
     mats = (gate_matrix, up_matrix, down_matrix)
-    edge, weights = pl.pallas_call(
-        edge_kernel,
-        grid=(1,),
-        in_specs=[
-            pl.BlockSpec((EDGE, a.shape[1]), lambda i: (length // EDGE - 1, 0)) for a in rowed
-        ]
-        + [fixed(a) for a in mats],
-        out_specs=[
-            pl.BlockSpec((EDGE, span), lambda i: (0, 0)),
-            pl.BlockSpec((mats[0].shape[0], 3 * mats[0].shape[1]), lambda i: (0, 0)),
-        ],
-        out_shape=[
-            struct((EDGE, span), BF16),
-            struct((mats[0].shape[0], 3 * mats[0].shape[1]), BF16),
-        ],
-        compiler_params=params(),
-        cost_estimate=cost(1e6, 1e6),
-    )(*rowed, *mats)
-    rim = lax.ppermute(edge, "sp", [(i, i + 1) for i in range(sp - 1)])
-
+    weights = joined(mats, [fixed(a) for a in mats])
     gain, ff_gain = head_norm_gain.reshape(1, inner), feedforward_norm_gain.reshape(1, width)
-    rim, gain, ff_gain = lax.optimization_barrier((rim, gain, ff_gain))
+    rim, gain, ff_gain, weights = lax.optimization_barrier((rim, gain, ff_gain, weights))
+    rim = pltpu.with_memory_space_constraint(rim, pltpu.HBM)
     row_spec = lambda w: pl.BlockSpec((BT, w), lambda i: (i, 0))
+    planes = lambda w: pltpu.VMEM((w // LANES, EDGE + BT, LANES), F32)
     time_spec = pl.BlockSpec((heads, BT), lambda i: (0, i))
     rate = log_decay_rate.reshape(1, heads)
     up, kk, er, eR, hs, st = pl.pallas_call(
@@ -456,17 +471,17 @@
             fixed(narrow_key_kernel), fixed(table), fixed(place), fixed(pick),
         ],
         out_specs=[
-            row_spec(inner), row_spec(keys), row_spec(heads), row_spec(heads),
+            row_spec(inner), row_spec(keys), row_spec(2 * heads), row_spec(2 * heads),
             pl.BlockSpec((1, rows, GW), lambda i: (i, 0, 0)),
             pl.BlockSpec((near * padded, GW), lambda i: (0, 0)),
         ],
         out_shape=[
             struct((length, inner), BF16), struct((length, keys), BF16),
-            struct((length, heads), F32), struct((length, heads), F32),
+            struct((length, 2 * heads), BF16), struct((length, 2 * heads), BF16),
             struct((blocks, rows, GW), BF16), struct((near * padded, GW), BF16),
         ],
         scratch_shapes=[
-            pltpu.VMEM((EDGE + BT, inner), F32), pltpu.VMEM((EDGE + BT, keys), F32),
+            planes(inner), planes(keys),
             pltpu.VMEM((rows, GW), F32), pltpu.VMEM((heads, BT), F32),
         ],
         compiler_params=params(),
@@ -477,30 +492,26 @@
         pick,
     )
 
+    weights, st = lax.optimization_barrier((weights, st))
+    weights = lax.all_gather(weights, "sp", axis=0, tiled=True)
+    weights = pltpu.with_memory_space_constraint(weights, pltpu.HBM)
     seats = [[q + n for n in range(near)] for q in range(0, sp, near)]
     exchange = lambda a: lax.all_to_all(a, "sp", 0, 0, axis_index_groups=seats, tiled=True)
     got = exchange(st)
-    yl, qq = pl.pallas_call(
+    inner_call = pl.pallas_call(
         functools.partial(inner_kernel, groups),
         grid=(blocks,),
         in_specs=[
             fixed(rim), row_spec(wcols), row_spec(ncols), fixed(wide_query_kernel),
-            fixed(narrow_query_kernel), row_spec(keys), row_spec(inner), row_spec(heads),
+            fixed(narrow_query_kernel), row_spec(keys), row_spec(inner), row_spec(2 * heads),
             pl.BlockSpec((1, rows, GW), lambda i: (i, 0, 0)), fixed(table),
         ],
         out_specs=[row_spec(inner), row_spec(keys)],
         out_shape=[struct((length, inner), F32), struct((length, keys), BF16)],
-        scratch_shapes=[pltpu.VMEM((EDGE + BT, keys), F32)],
+        scratch_shapes=[planes(keys)],
         compiler_params=params(),
         cost_estimate=cost(8e9, 6e6),
-    )(
-        rim, wide_query_rows, narrow_query_rows, wide_query_kernel, narrow_query_kernel, kk, up,
-        er, hs, table,
-    )
-    got, yl = lax.optimization_barrier((got, yl))
-    far = [
-        pltpu.with_memory_space_constraint(a, pltpu.HBM) for a in (yl, qq, eR, gate_projected, output_matrix)
-    ]
+    )
     smem = pl.BlockSpec(memory_space=pltpu.SMEM)
     vmem = pl.BlockSpec(memory_space=pltpu.VMEM)
     seat = lax.rem(me_sp, near).reshape(1)
@@ -515,9 +526,6 @@
         lax.ppermute(sent, "sp", [(i, i + near * n) for i in range(sp - near * n)])
         for n in range(1, sp // near)
     ]
-    weights, *others = lax.optimization_barrier((weights, *others))
-    weights = lax.all_gather(weights, "sp", axis=0, tiled=True)
-    weights = pltpu.with_memory_space_constraint(weights, pltpu.HBM)
     entered = pl.pallas_call(
         functools.partial(far_kernel, groups, chunk),
         in_specs=[smem] + [vmem] * (4 + len(others)),
@@ -525,7 +533,15 @@
         compiler_params=pltpu.CompilerParams(vmem_limit_bytes=SMALL_LIMIT),
         cost_estimate=cost(1e9, 1e6),
     )(seat, prefix, sums, unplace, table, *others)
+    er, entered = lax.optimization_barrier((er, entered))
     back = exchange(entered)
+    yl, qq = inner_call(
+        rim, wide_query_rows, narrow_query_rows, wide_query_kernel, narrow_query_kernel, kk, up,
+        er, hs, table,
+    )
+    far = [
+        pltpu.with_memory_space_constraint(a, pltpu.HBM) for a in (yl, qq, eR, gate_projected, output_matrix)
+    ]
     hin = whole(place_kernel, struct((rows, GW), BF16), unpick, back)
 
     share = length // tp
@@ -542,7 +558,7 @@
             grid_spec=pltpu.PrefetchScalarGridSpec(
                 num_scalar_prefetch=1,
                 grid=(width // tile,),
-                in_specs=[mine(w, n) for n in range(count) for w in (inner, keys, heads, inner)]
+                in_specs=[mine(w, n) for n in range(count) for w in (inner, keys, 2 * heads, inner)]
                 + [fixed(hin), fixed(gain), pl.BlockSpec((inner, tile), lambda i, o: (0, i))]
                 + [fixed(table), fixed(table_t)],
                 out_specs=[pl.BlockSpec((half, tile), lambda i, o: (0, i))] * (2 * count),

time: 204 us -> 197 us (0.966)
  waiting for transfers between devices: 46.6 us -> 41.6 us
  Pallas kernels: 66 us -> 63.4 us
    ppermute x18, waiting for transfers between devices: 29.7 us -> 23.5 us  [ring(): lax.ppermute(value, axis, [(i, (i + step) % count) for i in range(count)])]
    all_to_all x2, waiting for transfers between devices: 11 us -> 14.9 us  [on_device(): lax.all_to_all(a, 'sp', 0, 0, axis_index_groups=seats, tiled=True)]
    pallas_call x2 -> x3, Pallas kernels: 9.86 us -> 10.4 us  [the longest x1 7.31 us: on_device(): inner_call(rim, wide_query_rows, narrow_query_rows, wide_query_kernel, na...]
  transfers between devices with their start and end apart: 25 -> 25, of which waited for: 15 -> 13; matrix products, arithmetic and copies ran while one was open for 0% -> 0% of each run, Pallas kernels for 25% -> 26%
where the time goes in v1:
time: 197 us; the launch traced here: 194 us
  starting transfers between devices  74 us (38%)
  Pallas kernels  63.4 us (32%)
  waiting for transfers between devices  41.6 us (21%)
  between operations  13.7 us (7%)
    ppermute x18, starting transfers between devices, ring(): lax.ppermute(value, axis, [(i, (i + step) % count) for i in range(count)])  28.3 us
    ppermute x3, starting transfers between devices, on_device(): lax.ppermute(sent, 'sp', [(i, i + near * n) for i in range(sp - near * n)])  28 us
    ppermute x18, waiting for transfers between devices, ring(): lax.ppermute(value, axis, [(i, (i + step) % count) for i in range(count)])  23.5 us
    pallas_call x3, Pallas kernels, feed(): pl.pallas_call(functools.partial(feed_kernel, len(xs)), grid=(tiles,), in...  19.7 us
    pallas_call x3, Pallas kernels, project(): pl.pallas_call(functools.partial(project_kernel, groups, count), grid_spe...  18.8 us
    all_to_all x2, starting transfers between devices, on_device(): lax.all_to_all(a, 'sp', 0, 0, axis_index_groups=seats, tiled=True)  15.9 us
    all_to_all x2, waiting for transfers between devices, on_device(): lax.all_to_all(a, 'sp', 0, 0, axis_index_groups=seats, tiled=True)  14.9 us
    pallas_call x1, Pallas kernels, on_device(): pl.pallas_call(functools.partial(states_kernel, groups, chunk), grid=(blo...  9.87 us
  transfers between devices with their start and end apart: 25, of which 13 were waited for; matrix products, arithmetic and copies ran while one was open for 0% of the time, Pallas kernels for 26%

profile of v1, /device:TPU:38, one launch (start us, length us, event | category | flops | bytes accessed | tf_op | source)
XLA Modules:
  0.0 194.1 jit_solution(16301447213045735113)
XLA Ops:
  7.9 1.8 collective-permute-start
  9.8 1.7 shard_map.263
  12.2 9.9 %shard_map.264 = (bf16[768,1024]{1,0:T(8,128)(2,1)}, bf16[768,384]{1,0:T(8,128)(2,1)}, bf16[768,32]{1,0:T(8,128)(2,1)}, bf16[768,32]{1,0:T(8,128)(2,1)}, bf16[6,...) custom-call(bf16[8,1792]{1,0:T(8,128)(2,1)} %copy-done.12, bf16[768,1024]{1,0:T(8,128)(2,1)} %value.1, ...), custom_call_target="tpu_custom_call" | custom-call | flops 8000000000 | bytes 6000000 | tf_op jit(solution)/shard_map/pallas_call | solution.py:465
  22.1 12.3 %all-to-all-start = ((bf16[8,64,256]{2,1,0:T(8,128)(2,1)}), bf16[8,64,256]{2,1,0:T(8,128)(2,1)S(1)}, u32[]{:S(2)}, u32[]{:S(2)}) async-start(bf16[8,64,256]{2,1,0:T(8,128)(2,1)} %bitcast.11), calls=%async_computation | async-start | bytes 524288 | tf_op jit(solution)/shard_map/all_to_all | solution.py:499
  34.4 9.7 %all-to-all-done = bf16[8,64,256]{2,1,0:T(8,128)(2,1)S(1)} async-done(((bf16[8,64,256]{2,1,0:T(8,128)(2,1)}), bf16[8,64,256]{2,1,0:T(8,128)(2,1)S(1)}, u32[]{:S(2)}, u32[]{:S(2)}) %all-to-all-start) | async-done | bytes 262176 | tf_op jit(solution)/shard_map/all_to_all | solution.py:499
  44.7 12.6 %collective-permute-start.1 = (bf16[64,256]{1,0:T(8,128)(2,1)S(1)}, bf16[64,256]{1,0:T(8,128)(2,1)S(1)}, u32[]{:S(2)}, u32[]{:S(2)}) collective-permute-start(bf16[64,256]{1,0:T(8,128)(2,1)S(1)} %get-tuple-element.53), channel_id=1, source_target_pairs={{0,32},{4,36},{8,40},{12,44},{16,48},{20,52},{24,56},{28,60},{32,6... | collective-permute-start | bytes 98312 | tf_op jit(solution)/shard_map/ppermute | solution.py:526
  57.3 14.1 %collective-permute-start.2 = (bf16[64,256]{1,0:T(8,128)(2,1)S(1)}, bf16[64,256]{1,0:T(8,128)(2,1)S(1)}, u32[]{:S(2)}, u32[]{:S(2)}) collective-permute-start(bf16[64,256]{1,0:T(8,128)(2,1)S(1)} %get-tuple-element.53), channel_id=1, source_target_pairs={{0,64},{4,68},{8,72},{12,76},{16,80},{20,84},{24,88},{28,92},{32,9... | collective-permute-start | bytes 98312 | tf_op jit(solution)/shard_map/ppermute | solution.py:526
  73.3 2.6 %collective-permute-done.3.refs_2_ = bf16[64,256]{1,0:T(8,128)(2,1)S(1)} collective-permute-done((bf16[64,256]{1,0:T(8,128)(2,1)S(1)}, bf16[64,256]{1,0:T(8,128)(2,1)S(1)}, u32[]{:S(2)}, u32[]{:S(2)}) %collective-permute-start.3) | collective-permute-done | bytes 32800 | tf_op jit(solution)/shard_map/ppermute | solution.py:526
  77.2 3.6 %all-to-all-start.1 = ((bf16[8,64,256]{2,1,0:T(8,128)(2,1)}), bf16[8,64,256]{2,1,0:T(8,128)(2,1)S(1)}, u32[]{:S(2)}, u32[]{:S(2)}) async-start(bf16[8,64,256]{2,1,0:T(8,128)(2,1)} %bitcast.7), calls=%async_computation.1 | async-start | bytes 524288 | tf_op jit(solution)/shard_map/all_to_all | solution.py:499
  80.9 7.3 %shard_map.267 = (f32[768,1024]{1,0:T(8,128)}, bf16[768,384]{1,0:T(8,128)(2,1)}) custom-call(bf16[8,1792]{1,0:T(8,128)(2,1)} %copy-done.12, bf16[768,256]{1,0:T(8,128)(2,1)} %wq.1, bf16[768,128]{1,0:T(8,128)(2,1)} %nq.1, bf16[4,256]{1,0:T(4,128)(2,1)} %kwq.1, bf16[4,128]{1,0:T(4,128)(2,1)} %knq.1, bf16[768,384]{1,0:T(8,128)(2,1)} %get-tuple-element.45.kk, ...), custom_call_target="tpu_custom_call" | custom-call | flops 8000000000 | bytes 6000000 | tf_op jit(solution)/shard_map/pallas_call | solution.py:538
  88.2 5.2 %all-to-all-done.1 = bf16[8,64,256]{2,1,0:T(8,128)(2,1)S(1)} async-done(((bf16[8,64,256]{2,1,0:T(8,128)(2,1)}), bf16[8,64,256]{2,1,0:T(8,128)(2,1)S(1)}, u32[]{:S(2)}, u32[]{:S(2)}) %all-to-all-start.1) | async-done | bytes 262176 | tf_op jit(solution)/shard_map/all_to_all | solution.py:499
  93.7 5.5 %shard_map.271 = (bf16[96,2048]{1,0:T(8,128)(2,1)S(1)}, bf16[96,2048]{1,0:T(8,128)(2,1)S(1)}) custom-call(s32[1]{0:T(128)} %bitcast._, f32[768,1024]{1,0:T(8,128)} %get-tuple-element.56.refs_0_.refs_4_, bf16[768,384]{1,0:T(8,128)(2,1)} %get-tuple-element.57.refs_1_.refs_5_, bf16[768,32]{1,0:T(8,128)(2,1)} %get-tuple-element.58.refs_2_.refs_6_, ...), custom_call_target="tpu_custom_call" | custom-call | flops 805306368 | bytes 6000000 | tf_op jit(solution)/shard_map/pallas_call | solution.py:556
  99.4 2.0 %collective-permute-start.8 = (bf16[96,2048]{1,0:T(8,128)(2,1)S(1)}, bf16[96,2048]{1,0:T(8,128)(2,1)S(1)}, u32[]{:S(2)}, u32[]{:S(2)}) collective-permute-start(bf16[96,2048]{1,0:T(8,128)(2,1)S(1)} %get-tuple-element.70), channel_id=1, source_target_pairs={{0,3},{1,0},{2,1},{3,2},{4,7},{5,4},{6,5},{7,6},{8,11},{9,8},{10,9... | collective-permute-start | bytes 1179656 | tf_op jit(solution)/shard_map/ppermute | solution.py:360
  101.4 7.7 %shard_map.270 = (bf16[96,2048]{1,0:T(8,128)(2,1)S(1)}, bf16[96,2048]{1,0:T(8,128)(2,1)S(1)}, bf16[96,2048]{1,0:T(8,128)(2,1)S(1)}, bf16[96,2048]{1,0:T(8,128)(2,1)S(1)}) custom-call(s32[1]{0:T(128)} %bitcast._, f32[768,1024]{1,0:T(8,128)} %get-tuple-element.56.refs_0_.refs_4_, bf16[768,384]{1,0:T(8,128)(2,1)} %get-tuple-element.57.refs_1_.refs_5_, ...), custom_call_target="tpu_custom_call" | custom-call | flops 1610612736 | bytes 6000000 | tf_op jit(solution)/shard_map/pallas_call | solution.py:556
  109.8 2.8 %collective-permute-start.5 = (bf16[96,2048]{1,0:T(8,128)(2,1)S(1)}, bf16[96,2048]{1,0:T(8,128)(2,1)S(1)}, u32[]{:S(2)}, u32[]{:S(2)}) collective-permute-start(bf16[96,2048]{1,0:T(8,128)(2,1)S(1)} %shard_map.272), channel_id=1, source_target_pairs={{0,1},{1,2},{2,3},{3,0},{4,5},{5,6},{6,7},{7,4},{8,9},{9,10},{10,1... | collective-permute-start | bytes 1179656 | tf_op jit(solution)/shard_map/ppermute | solution.py:360
  112.9 2.2 %collective-permute-start.9 = (bf16[96,2048]{1,0:T(8,128)(2,1)S(1)}, bf16[96,2048]{1,0:T(8,128)(2,1)S(1)}, u32[]{:S(2)}, u32[]{:S(2)}) collective-permute-start(bf16[96,2048]{1,0:T(8,128)(2,1)S(1)} %shard_map.274), channel_id=1, source_target_pairs={{0,3},{1,0},{2,1},{3,2},{4,7},{5,4},{6,5},{7,6},{8,11},{9,8},{10,9... | collective-permute-start | bytes 1179656 | tf_op jit(solution)/shard_map/ppermute | solution.py:360
  115.1 5.5 %shard_map.269 = (bf16[96,2048]{1,0:T(8,128)(2,1)S(1)}, bf16[96,2048]{1,0:T(8,128)(2,1)S(1)}) custom-call(s32[1]{0:T(128)} %bitcast._, f32[768,1024]{1,0:T(8,128)} %get-tuple-element.56.refs_0_.refs_4_, bf16[768,384]{1,0:T(8,128)(2,1)} %get-tuple-element.57.refs_1_.refs_5_, bf16[768,32]{1,0:T(8,128)(2,1)} %get-tuple-element.58.refs_2_.refs_6_, ...), custom_call_target="tpu_custom_call" | custom-call | flops 805306368 | bytes 6000000 | tf_op jit(solution)/shard_map/pallas_call | solution.py:556
  120.6 1.8 collective-permute-done.6.two
  122.8 3.6 %collective-permute-start.10 = (bf16[96,2048]{1,0:T(8,128)(2,1)S(1)}, bf16[96,2048]{1,0:T(8,128)(2,1)S(1)}, u32[]{:S(2)}, u32[]{:S(2)}) collective-permute-start(bf16[96,2048]{1,0:T(8,128)(2,1)S(1)} %get-tuple-element.66.refs_0_), channel_id=1, source_target_pairs={{0,1},{1,2},{2,3},{3,0},{4,5},{5,6},{6,7},{7,4},{8,9},{9,10},{10,1... | collective-permute-start | bytes 1179656 | tf_op jit(solution)/shard_map/ppermute | solution.py:360
  126.4 4.2 %collective-permute-done.7.one = bf16[96,2048]{1,0:T(8,128)(2,1)S(1)} collective-permute-done((bf16[96,2048]{1,0:T(8,128)(2,1)S(1)}, bf16[96,2048]{1,0:T(8,128)(2,1)S(1)}, u32[]{:S(2)}, u32[]{:S(2)}) %collective-permute-start.7) | collective-permute-done | bytes 393248 | tf_op jit(solution)/shard_map/ppermute | solution.py:360
  132.0 4.3 %collective-permute-done.10.refs_0_ = bf16[96,2048]{1,0:T(8,128)(2,1)S(1)} collective-permute-done((bf16[96,2048]{1,0:T(8,128)(2,1)S(1)}, bf16[96,2048]{1,0:T(8,128)(2,1)S(1)}, u32[]{:S(2)}, u32[]{:S(2)}) %collective-permute-start.10) | collective-permute-done | bytes 393248 | tf_op jit(solution)/shard_map/ppermute | solution.py:360
  136.3 3.7 %collective-permute-start.14 = (bf16[96,2048]{1,0:T(8,128)(2,1)S(1)}, bf16[96,2048]{1,0:T(8,128)(2,1)S(1)}, u32[]{:S(2)}, u32[]{:S(2)}) collective-permute-start(bf16[96,2048]{1,0:T(8,128)(2,1)S(1)} %collective-permute-done.10.refs_0_), channel_id=1, source_target_pairs={{0,1},{1,2},{2,3},{3,0},{4,5},{5,6},{6,7},{7,4},{8,9},{9,10},{10,1... | collective-permute-start | bytes 1179656 | tf_op jit(solution)/shard_map/ppermute | solution.py:360
  141.8 4.7 %collective-permute-start.11 = (bf16[96,2048]{1,0:T(8,128)(2,1)S(1)}, bf16[96,2048]{1,0:T(8,128)(2,1)S(1)}, u32[]{:S(2)}, u32[]{:S(2)}) collective-permute-start(bf16[96,2048]{1,0:T(8,128)(2,1)S(1)} %get-tuple-element.71.refs_1_), channel_id=1, source_target_pairs={{0,1},{1,2},{2,3},{3,0},{4,5},{5,6},{6,7},{7,4},{8,9},{9,10},{10,1... | collective-permute-start | bytes 1179656 | tf_op jit(solution)/shard_map/ppermute | solution.py:360
  146.5 3.0 %collective-permute-done.14.refs_0_ = bf16[96,2048]{1,0:T(8,128)(2,1)S(1)} collective-permute-done((bf16[96,2048]{1,0:T(8,128)(2,1)S(1)}, bf16[96,2048]{1,0:T(8,128)(2,1)S(1)}, u32[]{:S(2)}, u32[]{:S(2)}) %collective-permute-start.14) | collective-permute-done | bytes 393248 | tf_op jit(solution)/shard_map/ppermute | solution.py:360
  149.5 4.4 %collective-permute-done.15.refs_1_ = bf16[96,2048]{1,0:T(8,128)(2,1)S(1)} collective-permute-done((bf16[96,2048]{1,0:T(8,128)(2,1)S(1)}, bf16[96,2048]{1,0:T(8,128)(2,1)S(1)}, u32[]{:S(2)}, u32[]{:S(2)}) %collective-permute-start.15) | collective-permute-done | bytes 393248 | tf_op jit(solution)/shard_map/ppermute | solution.py:360
  153.8 6.2 %shard_map.278 = (bf16[96,2048]{1,0:T(8,128)(2,1)S(1)}, bf16[96,2048]{1,0:T(8,128)(2,1)S(1)}) custom-call(bf16[96,2048]{1,0:T(8,128)(2,1)S(1)} %collective-permute-done.14.refs_0_, bf16[96,2048]{1,0:T(8,128)(2,1)S(1)} %collective-permute-done.15.refs_1_, bf16[2048,2304]{1,0:T(8,128)(2,1)} %all-gather.2.cloned.1.call-done.refs_2_.refs_3_.refs_4_.refs_5_.refs_6_, ...), custom_call_target="tpu_custom_call" | custom-call | flops 1811939328 | bytes 9437184 | tf_op jit(solution)/shard_map/pallas_call | solution.py:370
  160.0 2.1 %collective-permute-start.16 = (bf16[96,2048]{1,0:T(8,128)(2,1)S(1)}, bf16[96,2048]{1,0:T(8,128)(2,1)S(1)}, u32[]{:S(2)}, u32[]{:S(2)}) collective-permute-start(bf16[96,2048]{1,0:T(8,128)(2,1)S(1)} %get-tuple-element.75), channel_id=1, source_target_pairs={{0,1},{1,2},{2,3},{3,0},{4,5},{5,6},{6,7},{7,4},{8,9},{9,10},{10,1... | collective-permute-start | bytes 1179656 | tf_op jit(solution)/shard_map/ppermute | solution.py:360
  162.1 7.4 %shard_map.277 = (bf16[96,2048]{1,0:T(8,128)(2,1)S(1)}, bf16[96,2048]{1,0:T(8,128)(2,1)S(1)}, bf16[96,2048]{1,0:T(8,128)(2,1)S(1)}, bf16[96,2048]{1,0:T(8,128)(2,1)S(1)}) custom-call(bf16[96,2048]{1,0:T(8,128)(2,1)S(1)} %collective-permute-done.10.refs_0_, bf16[96,2048]{1,0:T(8,128)(2,1)S(1)} %collective-permute-done.11.refs_1_, ...), custom_call_target="tpu_custom_call" | custom-call | flops 3623878656 | bytes 9437184 | tf_op jit(solution)/shard_map/pallas_call | solution.py:370
  169.7 3.6 %collective-permute-start.19 = (bf16[96,2048]{1,0:T(8,128)(2,1)S(1)}, bf16[96,2048]{1,0:T(8,128)(2,1)S(1)}, u32[]{:S(2)}, u32[]{:S(2)}) collective-permute-start(bf16[96,2048]{1,0:T(8,128)(2,1)S(1)} %get-tuple-element.79), channel_id=1, source_target_pairs={{0,1},{1,2},{2,3},{3,0},{4,5},{5,6},{6,7},{7,4},{8,9},{9,10},{10,1... | collective-permute-start | bytes 1179656 | tf_op jit(solution)/shard_map/ppermute | solution.py:360
  173.3 1.8 collective-permute-start.17
  175.7 6.2 %shard_map.276 = (bf16[96,2048]{1,0:T(8,128)(2,1)S(1)}, bf16[96,2048]{1,0:T(8,128)(2,1)S(1)}) custom-call(bf16[96,2048]{1,0:T(8,128)(2,1)S(1)} %get-tuple-element.66.refs_0_, bf16[96,2048]{1,0:T(8,128)(2,1)S(1)} %get-tuple-element.71.refs_1_, bf16[2048,2304]{1,0:T(8,128)(2,1)} %all-gather.2.cloned.1.call-done.refs_2_.refs_3_.refs_4_.refs_5_.refs_6_, ...), custom_call_target="tpu_custom_call" | custom-call | flops 1811939328 | bytes 9437184 | tf_op jit(solution)/shard_map/pallas_call | solution.py:370
  181.9 2.8 %collective-permute-done.17.t1 = bf16[96,2048]{1,0:T(8,128)(2,1)S(1)} collective-permute-done((bf16[96,2048]{1,0:T(8,128)(2,1)S(1)}, bf16[96,2048]{1,0:T(8,128)(2,1)S(1)}, u32[]{:S(2)}, u32[]{:S(2)}) %collective-permute-start.17) | collective-permute-done | bytes 393248 | tf_op jit(solution)/shard_map/ppermute | solution.py:360
  (67 shorter events, 14.1 us)
Async XLA Ops:
  6.6 147.3 %all-gather.2.cloned.1.call-start = ((), (), s32[]{:S(2)}) async-start(), calls=%async_computation.2 | async-start | bytes 9732096 | tf_op jit(solution)/shard_map/all_gather | solution.py:496
  7.9 3.6 %collective-permute-start = (bf16[8,1792]{1,0:T(8,128)(2,1)}, bf16[8,1792]{1,0:T(8,128)(2,1)S(1)}, u32[]{:S(2)}, u32[]{:S(2)}) collective-permute-start(bf16[8,1792]{1,0:T(8,128)(2,1)} %shard_map.262), channel_id=1, source_target_pairs={{0,4},{4,8},{8,12},{12,16},{16,20},{20,24},{24,28},{28,32},{32,36}... | collective-permute-start | bytes 86024 | tf_op jit(solution)/shard_map/ppermute | solution.py:454
  12.2 32.0 %copy-start.1 = (bf16[32,1024]{1,0:T(8,128)(2,1)S(1)}, bf16[32,1024]{1,0:T(8,128)(2,1)}, u32[]{:S(2)}) copy-start(bf16[32,1024]{1,0:T(8,128)(2,1)} %constant.28.clone.table.refs_7_.refs_11_) | copy-start | bytes 196612
  12.2 32.0 %copy-start.7 = (bf16[256,16]{1,0:T(8,128)(2,1)S(1)}, bf16[256,16]{1,0:T(8,128)(2,1)}, u32[]{:S(2)}) copy-start(bf16[256,16]{1,0:T(8,128)(2,1)} %constant.31.clone.unplace) | copy-start | bytes 24580
  12.2 32.0 %copy-start.8 = (bf16[16,512]{1,0:T(8,128)(2,1)S(1)}, bf16[16,512]{1,0:T(8,128)(2,1)}, u32[]{:S(2)}) copy-start(bf16[16,512]{1,0:T(8,128)(2,1)} %constant.30.clone.place) | copy-start | bytes 49156
  12.2 32.0 %copy-start.9 = (bf16[8,512]{1,0:T(8,128)(2,1)S(1)}, bf16[8,512]{1,0:T(8,128)(2,1)}, u32[]{:S(2)}) copy-start(bf16[8,512]{1,0:T(8,128)(2,1)} %constant.34.clone.gather) | copy-start | bytes 24580
  22.1 22.0 %all-to-all-start = ((bf16[8,64,256]{2,1,0:T(8,128)(2,1)}), bf16[8,64,256]{2,1,0:T(8,128)(2,1)S(1)}, u32[]{:S(2)}, u32[]{:S(2)}) async-start(bf16[8,64,256]{2,1,0:T(8,128)(2,1)} %bitcast.11), calls=%async_computation | async-start | bytes 524288 | tf_op jit(solution)/shard_map/all_to_all | solution.py:499
  44.7 28.0 %collective-permute-start.1 = (bf16[64,256]{1,0:T(8,128)(2,1)S(1)}, bf16[64,256]{1,0:T(8,128)(2,1)S(1)}, u32[]{:S(2)}, u32[]{:S(2)}) collective-permute-start(bf16[64,256]{1,0:T(8,128)(2,1)S(1)} %get-tuple-element.53), channel_id=1, source_target_pairs={{0,32},{4,36},{8,40},{12,44},{16,48},{20,52},{24,56},{28,60},{32,6... | collective-permute-start | bytes 98312 | tf_op jit(solution)/shard_map/ppermute | solution.py:526
  57.3 16.0 %collective-permute-start.2 = (bf16[64,256]{1,0:T(8,128)(2,1)S(1)}, bf16[64,256]{1,0:T(8,128)(2,1)S(1)}, u32[]{:S(2)}, u32[]{:S(2)}) collective-permute-start(bf16[64,256]{1,0:T(8,128)(2,1)S(1)} %get-tuple-element.53), channel_id=1, source_target_pairs={{0,64},{4,68},{8,72},{12,76},{16,80},{20,84},{24,88},{28,92},{32,9... | collective-permute-start | bytes 98312 | tf_op jit(solution)/shard_map/ppermute | solution.py:526
  71.4 4.5 %collective-permute-start.3 = (bf16[64,256]{1,0:T(8,128)(2,1)S(1)}, bf16[64,256]{1,0:T(8,128)(2,1)S(1)}, u32[]{:S(2)}, u32[]{:S(2)}) collective-permute-start(bf16[64,256]{1,0:T(8,128)(2,1)S(1)} %get-tuple-element.53), channel_id=1, source_target_pairs={{0,96},{4,100},{8,104},{12,108},{16,112},{20,116},{24,120},{28,124... | collective-permute-start | bytes 98312 | tf_op jit(solution)/shard_map/ppermute | solution.py:526
  77.2 16.2 %all-to-all-start.1 = ((bf16[8,64,256]{2,1,0:T(8,128)(2,1)}), bf16[8,64,256]{2,1,0:T(8,128)(2,1)S(1)}, u32[]{:S(2)}, u32[]{:S(2)}) async-start(bf16[8,64,256]{2,1,0:T(8,128)(2,1)} %bitcast.7), calls=%async_computation.1 | async-start | bytes 524288 | tf_op jit(solution)/shard_map/all_to_all | solution.py:499
  80.9 12.5 %copy-start.3 = (bf16[384,512]{1,0:T(8,128)(2,1)S(1)}, bf16[384,512]{1,0:T(8,128)(2,1)}, u32[]{:S(2)}) copy-start(bf16[384,512]{1,0:T(8,128)(2,1)} %constant.33.clone.unpick) | copy-start | bytes 1179652
  80.9 12.8 %copy-start = (bf16[1024,16]{1,0:T(8,128)(2,1)S(1)}, bf16[1024,16]{1,0:T(8,128)(2,1)}, u32[]{:S(2)}) copy-start(bf16[1024,16]{1,0:T(8,128)(2,1)} %constant.29.clone.refs_8_.refs_12_) | copy-start | bytes 98308
  80.9 12.8 %copy-start.2 = (bf16[32,1024]{1,0:T(8,128)(2,1)S(1)}, bf16[32,1024]{1,0:T(8,128)(2,1)}, u32[]{:S(2)}) copy-start(bf16[32,1024]{1,0:T(8,128)(2,1)} %constant.28.clone.table.refs_7_.refs_11_) | copy-start | bytes 196612
  99.2 10.5 %collective-permute-start.4 = (bf16[96,2048]{1,0:T(8,128)(2,1)S(1)}, bf16[96,2048]{1,0:T(8,128)(2,1)S(1)}, u32[]{:S(2)}, u32[]{:S(2)}) collective-permute-start(bf16[96,2048]{1,0:T(8,128)(2,1)S(1)} %get-tuple-element.63), channel_id=1, source_target_pairs={{0,1},{1,2},{2,3},{3,0},{4,5},{5,6},{6,7},{7,4},{8,9},{9,10},{10,1... | collective-permute-start | bytes 1179656 | tf_op jit(solution)/shard_map/ppermute | solution.py:360
  99.4 13.4 %collective-permute-start.8 = (bf16[96,2048]{1,0:T(8,128)(2,1)S(1)}, bf16[96,2048]{1,0:T(8,128)(2,1)S(1)}, u32[]{:S(2)}, u32[]{:S(2)}) collective-permute-start(bf16[96,2048]{1,0:T(8,128)(2,1)S(1)} %get-tuple-element.70), channel_id=1, source_target_pairs={{0,3},{1,0},{2,1},{3,2},{4,7},{5,4},{6,5},{7,6},{8,11},{9,8},{10,9... | collective-permute-start | bytes 1179656 | tf_op jit(solution)/shard_map/ppermute | solution.py:360
  109.1 13.3 %collective-permute-start.6 = (bf16[96,2048]{1,0:T(8,128)(2,1)S(1)}, bf16[96,2048]{1,0:T(8,128)(2,1)S(1)}, u32[]{:S(2)}, u32[]{:S(2)}) collective-permute-start(bf16[96,2048]{1,0:T(8,128)(2,1)S(1)} %get-tuple-element.64), channel_id=1, source_target_pairs={{0,3},{1,0},{2,1},{3,2},{4,7},{5,4},{6,5},{7,6},{8,11},{9,8},{10,9... | collective-permute-start | bytes 1179656 | tf_op jit(solution)/shard_map/ppermute | solution.py:360
  109.8 12.6 %collective-permute-start.5 = (bf16[96,2048]{1,0:T(8,128)(2,1)S(1)}, bf16[96,2048]{1,0:T(8,128)(2,1)S(1)}, u32[]{:S(2)}, u32[]{:S(2)}) collective-permute-start(bf16[96,2048]{1,0:T(8,128)(2,1)S(1)} %shard_map.272), channel_id=1, source_target_pairs={{0,1},{1,2},{2,3},{3,0},{4,5},{5,6},{6,7},{7,4},{8,9},{9,10},{10,1... | collective-permute-start | bytes 1179656 | tf_op jit(solution)/shard_map/ppermute | solution.py:360
  112.7 17.9 %collective-permute-start.7 = (bf16[96,2048]{1,0:T(8,128)(2,1)S(1)}, bf16[96,2048]{1,0:T(8,128)(2,1)S(1)}, u32[]{:S(2)}, u32[]{:S(2)}) collective-permute-start(bf16[96,2048]{1,0:T(8,128)(2,1)S(1)} %get-tuple-element.68), channel_id=1, source_target_pairs={{0,1},{1,2},{2,3},{3,0},{4,5},{5,6},{6,7},{7,4},{8,9},{9,10},{10,1... | collective-permute-start | bytes 1179656 | tf_op jit(solution)/shard_map/ppermute | solution.py:360
  112.9 17.7 %collective-permute-start.9 = (bf16[96,2048]{1,0:T(8,128)(2,1)S(1)}, bf16[96,2048]{1,0:T(8,128)(2,1)S(1)}, u32[]{:S(2)}, u32[]{:S(2)}) collective-permute-start(bf16[96,2048]{1,0:T(8,128)(2,1)S(1)} %shard_map.274), channel_id=1, source_target_pairs={{0,3},{1,0},{2,1},{3,2},{4,7},{5,4},{6,5},{7,6},{8,11},{9,8},{10,9... | collective-permute-start | bytes 1179656 | tf_op jit(solution)/shard_map/ppermute | solution.py:360
  122.8 13.5 %collective-permute-start.10 = (bf16[96,2048]{1,0:T(8,128)(2,1)S(1)}, bf16[96,2048]{1,0:T(8,128)(2,1)S(1)}, u32[]{:S(2)}, u32[]{:S(2)}) collective-permute-start(bf16[96,2048]{1,0:T(8,128)(2,1)S(1)} %get-tuple-element.66.refs_0_), channel_id=1, source_target_pairs={{0,1},{1,2},{2,3},{3,0},{4,5},{5,6},{6,7},{7,4},{8,9},{9,10},{10,1... | collective-permute-start | bytes 1179656 | tf_op jit(solution)/shard_map/ppermute | solution.py:360
  131.7 9.8 %collective-permute-start.13 = (bf16[96,2048]{1,0:T(8,128)(2,1)S(1)}, bf16[96,2048]{1,0:T(8,128)(2,1)S(1)}, u32[]{:S(2)}, u32[]{:S(2)}) collective-permute-start(bf16[96,2048]{1,0:T(8,128)(2,1)S(1)} %get-tuple-element.71.refs_1_), channel_id=1, source_target_pairs={{0,3},{1,0},{2,1},{3,2},{4,7},{5,4},{6,5},{7,6},{8,11},{9,8},{10,9... | collective-permute-start | bytes 1179656 | tf_op jit(solution)/shard_map/ppermute | solution.py:360
  136.3 13.2 %collective-permute-start.14 = (bf16[96,2048]{1,0:T(8,128)(2,1)S(1)}, bf16[96,2048]{1,0:T(8,128)(2,1)S(1)}, u32[]{:S(2)}, u32[]{:S(2)}) collective-permute-start(bf16[96,2048]{1,0:T(8,128)(2,1)S(1)} %collective-permute-done.10.refs_0_), channel_id=1, source_target_pairs={{0,1},{1,2},{2,3},{3,0},{4,5},{5,6},{6,7},{7,4},{8,9},{9,10},{10,1... | collective-permute-start | bytes 1179656 | tf_op jit(solution)/shard_map/ppermute | solution.py:360
  141.5 12.3 %collective-permute-start.15 = (bf16[96,2048]{1,0:T(8,128)(2,1)S(1)}, bf16[96,2048]{1,0:T(8,128)(2,1)S(1)}, u32[]{:S(2)}, u32[]{:S(2)}) collective-permute-start(bf16[96,2048]{1,0:T(8,128)(2,1)S(1)} %collective-permute-done.13.refs_3_), channel_id=1, source_target_pairs={{0,3},{1,0},{2,1},{3,2},{4,7},{5,4},{6,5},{7,6},{8,11},{9,8},{10,9... | collective-permute-start | bytes 1179656 | tf_op jit(solution)/shard_map/ppermute | solution.py:360
  141.8 20.4 %collective-permute-start.11 = (bf16[96,2048]{1,0:T(8,128)(2,1)S(1)}, bf16[96,2048]{1,0:T(8,128)(2,1)S(1)}, u32[]{:S(2)}, u32[]{:S(2)}) collective-permute-start(bf16[96,2048]{1,0:T(8,128)(2,1)S(1)} %get-tuple-element.71.refs_1_), channel_id=1, source_target_pairs={{0,1},{1,2},{2,3},{3,0},{4,5},{5,6},{6,7},{7,4},{8,9},{9,10},{10,1... | collective-permute-start | bytes 1179656 | tf_op jit(solution)/shard_map/ppermute | solution.py:360
  146.5 15.6 %collective-permute-start.12 = (bf16[96,2048]{1,0:T(8,128)(2,1)S(1)}, bf16[96,2048]{1,0:T(8,128)(2,1)S(1)}, u32[]{:S(2)}, u32[]{:S(2)}) collective-permute-start(bf16[96,2048]{1,0:T(8,128)(2,1)S(1)} %get-tuple-element.66.refs_0_), channel_id=1, source_target_pairs={{0,3},{1,0},{2,1},{3,2},{4,7},{5,4},{6,5},{7,6},{8,11},{9,8},{10,9... | collective-permute-start | bytes 1179656 | tf_op jit(solution)/shard_map/ppermute | solution.py:360
  160.0 13.3 %collective-permute-start.16 = (bf16[96,2048]{1,0:T(8,128)(2,1)S(1)}, bf16[96,2048]{1,0:T(8,128)(2,1)S(1)}, u32[]{:S(2)}, u32[]{:S(2)}) collective-permute-start(bf16[96,2048]{1,0:T(8,128)(2,1)S(1)} %get-tuple-element.75), channel_id=1, source_target_pairs={{0,1},{1,2},{2,3},{3,0},{4,5},{5,6},{6,7},{7,4},{8,9},{9,10},{10,1... | collective-permute-start | bytes 1179656 | tf_op jit(solution)/shard_map/ppermute | solution.py:360
  162.1 13.2 %collective-permute-start.20 = (bf16[96,2048]{1,0:T(8,128)(2,1)S(1)}, bf16[96,2048]{1,0:T(8,128)(2,1)S(1)}, u32[]{:S(2)}, u32[]{:S(2)}) collective-permute-start(bf16[96,2048]{1,0:T(8,128)(2,1)S(1)} %get-tuple-element.81), channel_id=1, source_target_pairs={{0,3},{1,0},{2,1},{3,2},{4,7},{5,4},{6,5},{7,6},{8,11},{9,8},{10,9... | collective-permute-start | bytes 1179656 | tf_op jit(solution)/shard_map/ppermute | solution.py:360
  169.5 12.3 %collective-permute-start.18 = (bf16[96,2048]{1,0:T(8,128)(2,1)S(1)}, bf16[96,2048]{1,0:T(8,128)(2,1)S(1)}, u32[]{:S(2)}, u32[]{:S(2)}) collective-permute-start(bf16[96,2048]{1,0:T(8,128)(2,1)S(1)} %get-tuple-element.76), channel_id=1, source_target_pairs={{0,3},{1,0},{2,1},{3,2},{4,7},{5,4},{6,5},{7,6},{8,11},{9,8},{10,9... | collective-permute-start | bytes 1179656 | tf_op jit(solution)/shard_map/ppermute | solution.py:360
  169.7 12.2 %collective-permute-start.19 = (bf16[96,2048]{1,0:T(8,128)(2,1)S(1)}, bf16[96,2048]{1,0:T(8,128)(2,1)S(1)}, u32[]{:S(2)}, u32[]{:S(2)}) collective-permute-start(bf16[96,2048]{1,0:T(8,128)(2,1)S(1)} %get-tuple-element.79), channel_id=1, source_target_pairs={{0,1},{1,2},{2,3},{3,0},{4,5},{5,6},{6,7},{7,4},{8,9},{9,10},{10,1... | collective-permute-start | bytes 1179656 | tf_op jit(solution)/shard_map/ppermute | solution.py:360
  173.3 11.4 %collective-permute-start.17 = (bf16[96,2048]{1,0:T(8,128)(2,1)S(1)}, bf16[96,2048]{1,0:T(8,128)(2,1)S(1)}, u32[]{:S(2)}, u32[]{:S(2)}) collective-permute-start(bf16[96,2048]{1,0:T(8,128)(2,1)S(1)} %shard_map.279), channel_id=1, source_target_pairs={{0,1},{1,2},{2,3},{3,0},{4,5},{5,6},{6,7},{7,4},{8,9},{9,10},{10,1... | collective-permute-start | bytes 1179656 | tf_op jit(solution)/shard_map/ppermute | solution.py:360
  175.4 10.5 %collective-permute-start.21 = (bf16[96,2048]{1,0:T(8,128)(2,1)S(1)}, bf16[96,2048]{1,0:T(8,128)(2,1)S(1)}, u32[]{:S(2)}, u32[]{:S(2)}) collective-permute-start(bf16[96,2048]{1,0:T(8,128)(2,1)S(1)} %shard_map.280), channel_id=1, source_target_pairs={{0,3},{1,0},{2,1},{3,2},{4,7},{5,4},{6,5},{7,6},{8,11},{9,8},{10,9... | collective-permute-start | bytes 1179656 | tf_op jit(solution)/shard_map/ppermute | solution.py:360
  (6 other events, 27.9 us)
Sparse Core Ops, SparseCore 0:
  22.2 101.0 all-gather.1

commit v2 on v1

--- a/solution.py
+++ b/solution.py
@@ -255,33 +255,43 @@
 
 def project_kernel(groups, count, _, *refs):
     ins, (hin, gain, matrix, table, table_t) = refs[: 4 * count], refs[4 * count : 4 * count + 5]
-    outs, (held, normed) = refs[4 * count + 5 : -2], refs[-2:]
+    outs, (held, normed, near, arrived) = refs[4 * count + 5 : -4], refs[-4:]
     info, _ = group_rows(groups)
     share = ins[0].shape[0]
 
-    @pl.when(pl.program_id(0) == 0)
-    def _():
-        for n in range(count):
-            yl, qq, eR, gate = ins[4 * n : 4 * n + 4]
-            reach = eR[...]
-            squares = jnp.zeros((share, table.shape[0] // 2), F32)
-            for g, (row, size, key) in enumerate(info):
-                cols = slice(g * GW, (g + 1) * GW)
-                outer = dot(qq[:, key : key + size], hin[row : row + size, :])
-                y = yl[:, cols] + outer * dot(reach, table[:, cols])
-                gated = y * silu(gate[:, cols].astype(F32))
-                held[:, cols] = gated
-                squares += dot2(halves(gated * gated), table_t[cols, :])
-            scale = halves(lax.rsqrt(squares * (1.0 / CH) + EPS))
-            for g in range(groups):
-                cols = slice(g * GW, (g + 1) * GW)
-                unit = held[:, cols] * dot2(scale, table[: table.shape[0] // 2, cols]) * gain[:, cols].astype(F32)
-                normed[n * share : (n + 1) * share, cols] = unit.astype(BF16)
-
-    p = dot(normed[...], matrix[...]).astype(BF16)
+    tiles = arrived.shape[0]
+    tile = matrix.shape[1] // tiles
+    parts = [slice(t * tile, (t + 1) * tile) for t in range(tiles)]
+    copies = [
+        pltpu.make_async_copy(matrix.at[:, part], near.at[:, part], arrived.at[t])
+        for t, part in enumerate(parts)
+    ]
+    for copy in copies:
+        copy.start()
+    for n in range(count):
+        yl, qq, eR, gate = ins[4 * n : 4 * n + 4]
+        reach = eR[...]
+        squares = jnp.zeros((share, table.shape[0] // 2), F32)
+        for g, (row, size, key) in enumerate(info):
+            cols = slice(g * GW, (g + 1) * GW)
+            outer = dot(qq[:, key : key + size], hin[row : row + size, :])
+            y = yl[:, cols] + outer * dot(reach, table[:, cols])
+            gated = y * silu(gate[:, cols].astype(F32))
+            held[:, cols] = gated
+            squares += dot2(halves(gated * gated), table_t[cols, :])
+        scale = halves(lax.rsqrt(squares * (1.0 / CH) + EPS))
+        for g in range(groups):
+            cols = slice(g * GW, (g + 1) * GW)
+            spread = dot2(scale, table[: table.shape[0] // 2, cols])
+            unit = held[:, cols] * spread * gain[:, cols].astype(F32)
+            normed[n * share : (n + 1) * share, cols] = unit.astype(BF16)
+
     half = outs[0].shape[0]
-    for n, out in enumerate(outs):
-        out[...] = p[n * half : (n + 1) * half]
+    for copy, part in zip(copies, parts):
+        copy.wait()
+        p = dot(normed[...], near[:, part]).astype(BF16)
+        for n, out in enumerate(outs):
+            out[:, part] = p[n * half : (n + 1) * half]
 
 
 def place_kernel(unpick, back, out):
@@ -457,7 +467,6 @@
     weights = joined(mats, [fixed(a) for a in mats])
     gain, ff_gain = head_norm_gain.reshape(1, inner), feedforward_norm_gain.reshape(1, width)
     rim, gain, ff_gain, weights = lax.optimization_barrier((rim, gain, ff_gain, weights))
-    rim = pltpu.with_memory_space_constraint(rim, pltpu.HBM)
     row_spec = lambda w: pl.BlockSpec((BT, w), lambda i: (i, 0))
     planes = lambda w: pltpu.VMEM((w // LANES, EDGE + BT, LANES), F32)
     time_spec = pl.BlockSpec((heads, BT), lambda i: (0, i))
@@ -466,7 +475,7 @@
         functools.partial(states_kernel, groups, chunk),
         grid=(blocks,),
         in_specs=[
-            fixed(rim), row_spec(inner), row_spec(wcols), row_spec(ncols), time_spec,
+            pl.BlockSpec(memory_space=pltpu.VMEM), row_spec(inner), row_spec(wcols), row_spec(ncols), time_spec,
             time_spec, fixed(rate), fixed(value_kernel), fixed(wide_key_kernel),
             fixed(narrow_key_kernel), fixed(table), fixed(place), fixed(pick),
         ],
@@ -492,9 +501,6 @@
         pick,
     )
 
-    weights, st = lax.optimization_barrier((weights, st))
-    weights = lax.all_gather(weights, "sp", axis=0, tiled=True)
-    weights = pltpu.with_memory_space_constraint(weights, pltpu.HBM)
     seats = [[q + n for n in range(near)] for q in range(0, sp, near)]
     exchange = lambda a: lax.all_to_all(a, "sp", 0, 0, axis_index_groups=seats, tiled=True)
     got = exchange(st)
@@ -522,6 +528,9 @@
         compiler_params=pltpu.CompilerParams(vmem_limit_bytes=SMALL_LIMIT),
         cost_estimate=cost(1e9, 1e6),
     )(seat, got, gather, unplace, place, table)
+    weights, sent = lax.optimization_barrier((weights, sent))
+    weights = lax.all_gather(weights, "sp", axis=0, tiled=True)
+    weights = pltpu.with_memory_space_constraint(weights, pltpu.HBM)
     others = [
         lax.ppermute(sent, "sp", [(i, i + near * n) for i in range(sp - near * n)])
         for n in range(1, sp // near)
@@ -557,13 +566,14 @@
             functools.partial(project_kernel, groups, count),
             grid_spec=pltpu.PrefetchScalarGridSpec(
                 num_scalar_prefetch=1,
-                grid=(width // tile,),
+                grid=(1,),
                 in_specs=[mine(w, n) for n in range(count) for w in (inner, keys, 2 * heads, inner)]
-                + [fixed(hin), fixed(gain), pl.BlockSpec((inner, tile), lambda i, o: (0, i))]
+                + [fixed(hin), fixed(gain), pl.BlockSpec(memory_space=pltpu.HBM)]
                 + [fixed(table), fixed(table_t)],
-                out_specs=[pl.BlockSpec((half, tile), lambda i, o: (0, i))] * (2 * count),
+                out_specs=[pl.BlockSpec((half, width), lambda i, o: (0, 0))] * (2 * count),
                 scratch_shapes=[
-                    pltpu.VMEM((share, inner), F32), pltpu.VMEM((count * share, inner), BF16)
+                    pltpu.VMEM((share, inner), F32), pltpu.VMEM((count * share, inner), BF16),
+                    pltpu.VMEM((inner, width), BF16), pltpu.SemaphoreType.DMA((width // tile,)),
                 ],
             ),
             out_shape=[struct((half, width), BF16)] * (2 * count),

time: 197 us -> 195 us (0.990); the launches traced: 194 us -> 194 us
  waiting for transfers between devices: 41.6 us -> 50.7 us
  starting transfers between devices: 74 us -> 68.3 us
  Pallas kernels: 63.4 us -> 60 us
    ppermute x18, waiting for transfers between devices: 23.5 us -> 32 us  [ring(): lax.ppermute(value, axis, [(i, (i + step) % count) for i in range(count)])]
    ppermute x18, starting transfers between devices: 28.3 us -> 23.5 us  [ring(): lax.ppermute(value, axis, [(i, (i + step) % count) for i in range(count)])]
    pallas_call x3, Pallas kernels: 18.8 us -> 15.4 us  [project(): pl.pallas_call(functools.partial(project_kernel, groups, count), grid_spe...]
  transfers between devices with their start and end apart: 25 -> 25, of which waited for: 13 -> 15; matrix products, arithmetic and copies ran while one was open for 0% -> 0% of each run, Pallas kernels for 26% -> 24%
where the time goes in v2:
time: 195 us; the launch traced here: 194 us
  starting transfers between devices  68.3 us (35%)
  Pallas kernels  60 us (31%)
  waiting for transfers between devices  50.7 us (26%)
  between operations  13.7 us (7%)
    ppermute x18, waiting for transfers between devices, ring(): lax.ppermute(value, axis, [(i, (i + step) % count) for i in range(count)])  32 us
    ppermute x3, starting transfers between devices, on_device(): lax.ppermute(sent, 'sp', [(i, i + near * n) for i in range(sp - near * n)])  27 us
    ppermute x18, starting transfers between devices, ring(): lax.ppermute(value, axis, [(i, (i + step) % count) for i in range(count)])  23.5 us
    pallas_call x3, Pallas kernels, feed(): pl.pallas_call(functools.partial(feed_kernel, len(xs)), grid=(tiles,), in...  19.7 us
    all_to_all x2, starting transfers between devices, on_device(): lax.all_to_all(a, 'sp', 0, 0, axis_index_groups=seats, tiled=True)  15.9 us
    pallas_call x3, Pallas kernels, project(): pl.pallas_call(functools.partial(project_kernel, groups, count), grid_spe...  15.4 us
    all_to_all x2, waiting for transfers between devices, on_device(): lax.all_to_all(a, 'sp', 0, 0, axis_index_groups=seats, tiled=True)  14.4 us
    pallas_call x1, Pallas kernels, on_device(): pl.pallas_call(functools.partial(states_kernel, groups, chunk), grid=(blo...  9.87 us
  transfers between devices with their start and end apart: 25, of which 15 were waited for; matrix products, arithmetic and copies ran while one was open for 0% of the time, Pallas kernels for 24%

profile of v2, /device:TPU:38, one launch (start us, length us, event | category | flops | bytes accessed | tf_op | source)
XLA Modules:
  0.0 194.2 jit_solution(7071458924234158828)
XLA Ops:
  6.6 1.4 shard_map.262
  7.9 1.8 collective-permute-start
  9.8 1.7 shard_map.263
  12.2 9.9 %shard_map.264 = (bf16[768,1024]{1,0:T(8,128)(2,1)}, bf16[768,384]{1,0:T(8,128)(2,1)}, bf16[768,32]{1,0:T(8,128)(2,1)}, bf16[768,32]{1,0:T(8,128)(2,1)}, bf16[6,...) custom-call(bf16[8,1792]{1,0:T(8,128)(2,1)} %copy-done.12, bf16[768,1024]{1,0:T(8,128)(2,1)} %value.1, ...), custom_call_target="tpu_custom_call" | custom-call | flops 8000000000 | bytes 6000000 | tf_op jit(solution)/shard_map/pallas_call | solution.py:474
  22.0 12.3 %all-to-all-start = ((bf16[8,64,256]{2,1,0:T(8,128)(2,1)}), bf16[8,64,256]{2,1,0:T(8,128)(2,1)S(1)}, u32[]{:S(2)}, u32[]{:S(2)}) async-start(bf16[8,64,256]{2,1,0:T(8,128)(2,1)} %bitcast.11), calls=%async_computation | async-start | bytes 524288 | tf_op jit(solution)/shard_map/all_to_all | solution.py:505
  34.4 9.6 %all-to-all-done = bf16[8,64,256]{2,1,0:T(8,128)(2,1)S(1)} async-done(((bf16[8,64,256]{2,1,0:T(8,128)(2,1)}), bf16[8,64,256]{2,1,0:T(8,128)(2,1)S(1)}, u32[]{:S(2)}, u32[]{:S(2)}) %all-to-all-start) | async-done | bytes 262176 | tf_op jit(solution)/shard_map/all_to_all | solution.py:505
  44.7 12.6 %collective-permute-start.1 = (bf16[64,256]{1,0:T(8,128)(2,1)S(1)}, bf16[64,256]{1,0:T(8,128)(2,1)S(1)}, u32[]{:S(2)}, u32[]{:S(2)}) collective-permute-start(bf16[64,256]{1,0:T(8,128)(2,1)S(1)} %get-tuple-element.53), channel_id=1, source_target_pairs={{0,32},{4,36},{8,40},{12,44},{16,48},{20,52},{24,56},{28,60},{32,6... | collective-permute-start | bytes 98312 | tf_op jit(solution)/shard_map/ppermute | solution.py:535
  57.3 13.1 %collective-permute-start.2 = (bf16[64,256]{1,0:T(8,128)(2,1)S(1)}, bf16[64,256]{1,0:T(8,128)(2,1)S(1)}, u32[]{:S(2)}, u32[]{:S(2)}) collective-permute-start(bf16[64,256]{1,0:T(8,128)(2,1)S(1)} %get-tuple-element.53), channel_id=1, source_target_pairs={{0,64},{4,68},{8,72},{12,76},{16,80},{20,84},{24,88},{28,92},{32,9... | collective-permute-start | bytes 98312 | tf_op jit(solution)/shard_map/ppermute | solution.py:535
  72.0 4.0 %collective-permute-done.3.refs_2_ = bf16[64,256]{1,0:T(8,128)(2,1)S(1)} collective-permute-done((bf16[64,256]{1,0:T(8,128)(2,1)S(1)}, bf16[64,256]{1,0:T(8,128)(2,1)S(1)}, u32[]{:S(2)}, u32[]{:S(2)}) %collective-permute-start.3) | collective-permute-done | bytes 32800 | tf_op jit(solution)/shard_map/ppermute | solution.py:535
  77.3 3.6 %all-to-all-start.1 = ((bf16[8,64,256]{2,1,0:T(8,128)(2,1)}), bf16[8,64,256]{2,1,0:T(8,128)(2,1)S(1)}, u32[]{:S(2)}, u32[]{:S(2)}) async-start(bf16[8,64,256]{2,1,0:T(8,128)(2,1)} %bitcast.7), calls=%async_computation.1 | async-start | bytes 524288 | tf_op jit(solution)/shard_map/all_to_all | solution.py:505
  81.0 7.3 %shard_map.267 = (f32[768,1024]{1,0:T(8,128)}, bf16[768,384]{1,0:T(8,128)(2,1)}) custom-call(bf16[8,1792]{1,0:T(8,128)(2,1)} %copy-done.12, bf16[768,256]{1,0:T(8,128)(2,1)} %wq.1, bf16[768,128]{1,0:T(8,128)(2,1)} %nq.1, bf16[4,256]{1,0:T(4,128)(2,1)} %kwq.1, bf16[4,128]{1,0:T(4,128)(2,1)} %knq.1, bf16[768,384]{1,0:T(8,128)(2,1)} %get-tuple-element.45.kk, ...), custom_call_target="tpu_custom_call" | custom-call | flops 8000000000 | bytes 6000000 | tf_op jit(solution)/shard_map/pallas_call | solution.py:547
  88.3 4.7 %all-to-all-done.1 = bf16[8,64,256]{2,1,0:T(8,128)(2,1)S(1)} async-done(((bf16[8,64,256]{2,1,0:T(8,128)(2,1)}), bf16[8,64,256]{2,1,0:T(8,128)(2,1)S(1)}, u32[]{:S(2)}, u32[]{:S(2)}) %all-to-all-start.1) | async-done | bytes 262176 | tf_op jit(solution)/shard_map/all_to_all | solution.py:505
  93.3 4.2 %shard_map.271 = (bf16[96,2048]{1,0:T(8,128)(2,1)S(1)}, bf16[96,2048]{1,0:T(8,128)(2,1)S(1)}) custom-call(s32[1]{0:T(128)} %bitcast._, f32[768,1024]{1,0:T(8,128)} %get-tuple-element.56.refs_0_.refs_4_, bf16[768,384]{1,0:T(8,128)(2,1)} %get-tuple-element.57.refs_1_.refs_5_, bf16[768,32]{1,0:T(8,128)(2,1)} %get-tuple-element.58.refs_2_.refs_6_, ...), custom_call_target="tpu_custom_call" | custom-call | flops 805306368 | bytes 6000000 | tf_op jit(solution)/shard_map/pallas_call | solution.py:565
  97.7 2.0 %collective-permute-start.8 = (bf16[96,2048]{1,0:T(8,128)(2,1)S(1)}, bf16[96,2048]{1,0:T(8,128)(2,1)S(1)}, u32[]{:S(2)}, u32[]{:S(2)}) collective-permute-start(bf16[96,2048]{1,0:T(8,128)(2,1)S(1)} %get-tuple-element.70), channel_id=1, source_target_pairs={{0,3},{1,0},{2,1},{3,2},{4,7},{5,4},{6,5},{7,6},{8,11},{9,8},{10,9... | collective-permute-start | bytes 1179656 | tf_op jit(solution)/shard_map/ppermute | solution.py:370
  99.7 7.0 %shard_map.270 = (bf16[96,2048]{1,0:T(8,128)(2,1)S(1)}, bf16[96,2048]{1,0:T(8,128)(2,1)S(1)}, bf16[96,2048]{1,0:T(8,128)(2,1)S(1)}, bf16[96,2048]{1,0:T(8,128)(2,1)S(1)}) custom-call(s32[1]{0:T(128)} %bitcast._, f32[768,1024]{1,0:T(8,128)} %get-tuple-element.56.refs_0_.refs_4_, bf16[768,384]{1,0:T(8,128)(2,1)} %get-tuple-element.57.refs_1_.refs_5_, ...), custom_call_target="tpu_custom_call" | custom-call | flops 1610612736 | bytes 6000000 | tf_op jit(solution)/shard_map/pallas_call | solution.py:565
  108.6 1.8 collective-permute-start.5
  110.7 2.0 %collective-permute-start.9 = (bf16[96,2048]{1,0:T(8,128)(2,1)S(1)}, bf16[96,2048]{1,0:T(8,128)(2,1)S(1)}, u32[]{:S(2)}, u32[]{:S(2)}) collective-permute-start(bf16[96,2048]{1,0:T(8,128)(2,1)S(1)} %shard_map.274), channel_id=1, source_target_pairs={{0,3},{1,0},{2,1},{3,2},{4,7},{5,4},{6,5},{7,6},{8,11},{9,8},{10,9... | collective-permute-start | bytes 1179656 | tf_op jit(solution)/shard_map/ppermute | solution.py:370
  112.6 4.2 %shard_map.269 = (bf16[96,2048]{1,0:T(8,128)(2,1)S(1)}, bf16[96,2048]{1,0:T(8,128)(2,1)S(1)}) custom-call(s32[1]{0:T(128)} %bitcast._, f32[768,1024]{1,0:T(8,128)} %get-tuple-element.56.refs_0_.refs_4_, bf16[768,384]{1,0:T(8,128)(2,1)} %get-tuple-element.57.refs_1_.refs_5_, bf16[768,32]{1,0:T(8,128)(2,1)} %get-tuple-element.58.refs_2_.refs_6_, ...), custom_call_target="tpu_custom_call" | custom-call | flops 805306368 | bytes 6000000 | tf_op jit(solution)/shard_map/pallas_call | solution.py:565
  116.9 3.1 %collective-permute-done.6.two = bf16[96,2048]{1,0:T(8,128)(2,1)S(1)} collective-permute-done((bf16[96,2048]{1,0:T(8,128)(2,1)S(1)}, bf16[96,2048]{1,0:T(8,128)(2,1)S(1)}, u32[]{:S(2)}, u32[]{:S(2)}) %collective-permute-start.6) | collective-permute-done | bytes 393248 | tf_op jit(solution)/shard_map/ppermute | solution.py:370
  121.3 2.8 %collective-permute-start.10 = (bf16[96,2048]{1,0:T(8,128)(2,1)S(1)}, bf16[96,2048]{1,0:T(8,128)(2,1)S(1)}, u32[]{:S(2)}, u32[]{:S(2)}) collective-permute-start(bf16[96,2048]{1,0:T(8,128)(2,1)S(1)} %get-tuple-element.66.refs_0_), channel_id=1, source_target_pairs={{0,1},{1,2},{2,3},{3,0},{4,5},{5,6},{6,7},{7,4},{8,9},{9,10},{10,1... | collective-permute-start | bytes 1179656 | tf_op jit(solution)/shard_map/ppermute | solution.py:370
  124.1 5.2 %collective-permute-done.7.one = bf16[96,2048]{1,0:T(8,128)(2,1)S(1)} collective-permute-done((bf16[96,2048]{1,0:T(8,128)(2,1)S(1)}, bf16[96,2048]{1,0:T(8,128)(2,1)S(1)}, u32[]{:S(2)}, u32[]{:S(2)}) %collective-permute-start.7) | collective-permute-done | bytes 393248 | tf_op jit(solution)/shard_map/ppermute | solution.py:370
  130.4 5.4 %collective-permute-done.10.refs_0_ = bf16[96,2048]{1,0:T(8,128)(2,1)S(1)} collective-permute-done((bf16[96,2048]{1,0:T(8,128)(2,1)S(1)}, bf16[96,2048]{1,0:T(8,128)(2,1)S(1)}, u32[]{:S(2)}, u32[]{:S(2)}) %collective-permute-start.10) | collective-permute-done | bytes 393248 | tf_op jit(solution)/shard_map/ppermute | solution.py:370
  135.9 3.0 %collective-permute-start.14 = (bf16[96,2048]{1,0:T(8,128)(2,1)S(1)}, bf16[96,2048]{1,0:T(8,128)(2,1)S(1)}, u32[]{:S(2)}, u32[]{:S(2)}) collective-permute-start(bf16[96,2048]{1,0:T(8,128)(2,1)S(1)} %collective-permute-done.10.refs_0_), channel_id=1, source_target_pairs={{0,1},{1,2},{2,3},{3,0},{4,5},{5,6},{6,7},{7,4},{8,9},{9,10},{10,1... | collective-permute-start | bytes 1179656 | tf_op jit(solution)/shard_map/ppermute | solution.py:370
  139.5 3.2 %collective-permute-start.11 = (bf16[96,2048]{1,0:T(8,128)(2,1)S(1)}, bf16[96,2048]{1,0:T(8,128)(2,1)S(1)}, u32[]{:S(2)}, u32[]{:S(2)}) collective-permute-start(bf16[96,2048]{1,0:T(8,128)(2,1)S(1)} %get-tuple-element.71.refs_1_), channel_id=1, source_target_pairs={{0,1},{1,2},{2,3},{3,0},{4,5},{5,6},{6,7},{7,4},{8,9},{9,10},{10,1... | collective-permute-start | bytes 1179656 | tf_op jit(solution)/shard_map/ppermute | solution.py:370
  142.7 5.6 %collective-permute-done.14.refs_0_ = bf16[96,2048]{1,0:T(8,128)(2,1)S(1)} collective-permute-done((bf16[96,2048]{1,0:T(8,128)(2,1)S(1)}, bf16[96,2048]{1,0:T(8,128)(2,1)S(1)}, u32[]{:S(2)}, u32[]{:S(2)}) %collective-permute-start.14) | collective-permute-done | bytes 393248 | tf_op jit(solution)/shard_map/ppermute | solution.py:370
  148.4 4.3 %collective-permute-done.15.refs_1_ = bf16[96,2048]{1,0:T(8,128)(2,1)S(1)} collective-permute-done((bf16[96,2048]{1,0:T(8,128)(2,1)S(1)}, bf16[96,2048]{1,0:T(8,128)(2,1)S(1)}, u32[]{:S(2)}, u32[]{:S(2)}) %collective-permute-start.15) | collective-permute-done | bytes 393248 | tf_op jit(solution)/shard_map/ppermute | solution.py:370
  152.7 6.1 %shard_map.278 = (bf16[96,2048]{1,0:T(8,128)(2,1)S(1)}, bf16[96,2048]{1,0:T(8,128)(2,1)S(1)}) custom-call(bf16[96,2048]{1,0:T(8,128)(2,1)S(1)} %collective-permute-done.14.refs_0_, bf16[96,2048]{1,0:T(8,128)(2,1)S(1)} %collective-permute-done.15.refs_1_, bf16[2048,2304]{1,0:T(8,128)(2,1)} %all-gather.2.cloned.1.call-done.refs_2_.refs_3_.refs_4_.refs_5_.refs_6_, ...), custom_call_target="tpu_custom_call" | custom-call | flops 1811939328 | bytes 9437184 | tf_op jit(solution)/shard_map/pallas_call | solution.py:380
  161.0 7.4 %shard_map.277 = (bf16[96,2048]{1,0:T(8,128)(2,1)S(1)}, bf16[96,2048]{1,0:T(8,128)(2,1)S(1)}, bf16[96,2048]{1,0:T(8,128)(2,1)S(1)}, bf16[96,2048]{1,0:T(8,128)(2,1)S(1)}) custom-call(bf16[96,2048]{1,0:T(8,128)(2,1)S(1)} %collective-permute-done.10.refs_0_, bf16[96,2048]{1,0:T(8,128)(2,1)S(1)} %collective-permute-done.11.refs_1_, ...), custom_call_target="tpu_custom_call" | custom-call | flops 3623878656 | bytes 9437184 | tf_op jit(solution)/shard_map/pallas_call | solution.py:380
  168.5 3.2 %collective-permute-start.19 = (bf16[96,2048]{1,0:T(8,128)(2,1)S(1)}, bf16[96,2048]{1,0:T(8,128)(2,1)S(1)}, u32[]{:S(2)}, u32[]{:S(2)}) collective-permute-start(bf16[96,2048]{1,0:T(8,128)(2,1)S(1)} %get-tuple-element.79), channel_id=1, source_target_pairs={{0,1},{1,2},{2,3},{3,0},{4,5},{5,6},{6,7},{7,4},{8,9},{9,10},{10,1... | collective-permute-start | bytes 1179656 | tf_op jit(solution)/shard_map/ppermute | solution.py:370
  174.2 6.2 %shard_map.276 = (bf16[96,2048]{1,0:T(8,128)(2,1)S(1)}, bf16[96,2048]{1,0:T(8,128)(2,1)S(1)}) custom-call(bf16[96,2048]{1,0:T(8,128)(2,1)S(1)} %get-tuple-element.66.refs_0_, bf16[96,2048]{1,0:T(8,128)(2,1)S(1)} %get-tuple-element.71.refs_1_, bf16[2048,2304]{1,0:T(8,128)(2,1)} %all-gather.2.cloned.1.call-done.refs_2_.refs_3_.refs_4_.refs_5_.refs_6_, ...), custom_call_target="tpu_custom_call" | custom-call | flops 1811939328 | bytes 9437184 | tf_op jit(solution)/shard_map/pallas_call | solution.py:380
  181.7 1.9 collective-permute-done.17.t1
  183.6 2.4 %collective-permute-done.21.b2 = bf16[96,2048]{1,0:T(8,128)(2,1)S(1)} collective-permute-done((bf16[96,2048]{1,0:T(8,128)(2,1)S(1)}, bf16[96,2048]{1,0:T(8,128)(2,1)S(1)}, u32[]{:S(2)}, u32[]{:S(2)}) %collective-permute-start.21) | collective-permute-done | bytes 393248 | tf_op jit(solution)/shard_map/ppermute | solution.py:370
  (67 shorter events, 17.2 us)
Async XLA Ops:
  7.9 3.6 %collective-permute-start = (bf16[8,1792]{1,0:T(8,128)(2,1)}, bf16[8,1792]{1,0:T(8,128)(2,1)S(1)}, u32[]{:S(2)}, u32[]{:S(2)}) collective-permute-start(bf16[8,1792]{1,0:T(8,128)(2,1)} %shard_map.262), channel_id=1, source_target_pairs={{0,4},{4,8},{8,12},{12,16},{16,20},{20,24},{24,28},{28,32},{32,36}... | collective-permute-start | bytes 86024 | tf_op jit(solution)/shard_map/ppermute | solution.py:464
  12.2 31.9 %copy-start.1 = (bf16[32,1024]{1,0:T(8,128)(2,1)S(1)}, bf16[32,1024]{1,0:T(8,128)(2,1)}, u32[]{:S(2)}) copy-start(bf16[32,1024]{1,0:T(8,128)(2,1)} %constant.28.clone.table.refs_7_.refs_11_) | copy-start | bytes 196612
  12.2 31.9 %copy-start.7 = (bf16[256,16]{1,0:T(8,128)(2,1)S(1)}, bf16[256,16]{1,0:T(8,128)(2,1)}, u32[]{:S(2)}) copy-start(bf16[256,16]{1,0:T(8,128)(2,1)} %constant.31.clone.unplace) | copy-start | bytes 24580
  12.2 31.9 %copy-start.8 = (bf16[16,512]{1,0:T(8,128)(2,1)S(1)}, bf16[16,512]{1,0:T(8,128)(2,1)}, u32[]{:S(2)}) copy-start(bf16[16,512]{1,0:T(8,128)(2,1)} %constant.30.clone.place) | copy-start | bytes 49156
  12.2 31.9 %copy-start.9 = (bf16[8,512]{1,0:T(8,128)(2,1)S(1)}, bf16[8,512]{1,0:T(8,128)(2,1)}, u32[]{:S(2)}) copy-start(bf16[8,512]{1,0:T(8,128)(2,1)} %constant.34.clone.gather) | copy-start | bytes 24580
  22.0 22.0 %all-to-all-start = ((bf16[8,64,256]{2,1,0:T(8,128)(2,1)}), bf16[8,64,256]{2,1,0:T(8,128)(2,1)S(1)}, u32[]{:S(2)}, u32[]{:S(2)}) async-start(bf16[8,64,256]{2,1,0:T(8,128)(2,1)} %bitcast.11), calls=%async_computation | async-start | bytes 524288 | tf_op jit(solution)/shard_map/all_to_all | solution.py:505
  34.4 118.3 %all-gather.2.cloned.1.call-start = ((), (), s32[]{:S(2)}) async-start(), calls=%async_computation.2 | async-start | bytes 9732096 | tf_op jit(solution)/shard_map/all_gather | solution.py:532
  44.7 27.0 %collective-permute-start.1 = (bf16[64,256]{1,0:T(8,128)(2,1)S(1)}, bf16[64,256]{1,0:T(8,128)(2,1)S(1)}, u32[]{:S(2)}, u32[]{:S(2)}) collective-permute-start(bf16[64,256]{1,0:T(8,128)(2,1)S(1)} %get-tuple-element.53), channel_id=1, source_target_pairs={{0,32},{4,36},{8,40},{12,44},{16,48},{20,52},{24,56},{28,60},{32,6... | collective-permute-start | bytes 98312 | tf_op jit(solution)/shard_map/ppermute | solution.py:535
  57.3 14.7 %collective-permute-start.2 = (bf16[64,256]{1,0:T(8,128)(2,1)S(1)}, bf16[64,256]{1,0:T(8,128)(2,1)S(1)}, u32[]{:S(2)}, u32[]{:S(2)}) collective-permute-start(bf16[64,256]{1,0:T(8,128)(2,1)S(1)} %get-tuple-element.53), channel_id=1, source_target_pairs={{0,64},{4,68},{8,72},{12,76},{16,80},{20,84},{24,88},{28,92},{32,9... | collective-permute-start | bytes 98312 | tf_op jit(solution)/shard_map/ppermute | solution.py:535
  70.4 5.6 %collective-permute-start.3 = (bf16[64,256]{1,0:T(8,128)(2,1)S(1)}, bf16[64,256]{1,0:T(8,128)(2,1)S(1)}, u32[]{:S(2)}, u32[]{:S(2)}) collective-permute-start(bf16[64,256]{1,0:T(8,128)(2,1)S(1)} %get-tuple-element.53), channel_id=1, source_target_pairs={{0,96},{4,100},{8,104},{12,108},{16,112},{20,116},{24,120},{28,124... | collective-permute-start | bytes 98312 | tf_op jit(solution)/shard_map/ppermute | solution.py:535
  77.3 15.7 %all-to-all-start.1 = ((bf16[8,64,256]{2,1,0:T(8,128)(2,1)}), bf16[8,64,256]{2,1,0:T(8,128)(2,1)S(1)}, u32[]{:S(2)}, u32[]{:S(2)}) async-start(bf16[8,64,256]{2,1,0:T(8,128)(2,1)} %bitcast.7), calls=%async_computation.1 | async-start | bytes 524288 | tf_op jit(solution)/shard_map/all_to_all | solution.py:505
  81.0 12.3 %copy-start = (bf16[1024,16]{1,0:T(8,128)(2,1)S(1)}, bf16[1024,16]{1,0:T(8,128)(2,1)}, u32[]{:S(2)}) copy-start(bf16[1024,16]{1,0:T(8,128)(2,1)} %constant.29.clone.refs_8_.refs_12_) | copy-start | bytes 98308
  81.0 12.3 %copy-start.2 = (bf16[32,1024]{1,0:T(8,128)(2,1)S(1)}, bf16[32,1024]{1,0:T(8,128)(2,1)}, u32[]{:S(2)}) copy-start(bf16[32,1024]{1,0:T(8,128)(2,1)} %constant.28.clone.table.refs_7_.refs_11_) | copy-start | bytes 196612
  97.5 11.0 %collective-permute-start.4 = (bf16[96,2048]{1,0:T(8,128)(2,1)S(1)}, bf16[96,2048]{1,0:T(8,128)(2,1)S(1)}, u32[]{:S(2)}, u32[]{:S(2)}) collective-permute-start(bf16[96,2048]{1,0:T(8,128)(2,1)S(1)} %get-tuple-element.63), channel_id=1, source_target_pairs={{0,1},{1,2},{2,3},{3,0},{4,5},{5,6},{6,7},{7,4},{8,9},{9,10},{10,1... | collective-permute-start | bytes 1179656 | tf_op jit(solution)/shard_map/ppermute | solution.py:370
  97.7 12.9 %collective-permute-start.8 = (bf16[96,2048]{1,0:T(8,128)(2,1)S(1)}, bf16[96,2048]{1,0:T(8,128)(2,1)S(1)}, u32[]{:S(2)}, u32[]{:S(2)}) collective-permute-start(bf16[96,2048]{1,0:T(8,128)(2,1)S(1)} %get-tuple-element.70), channel_id=1, source_target_pairs={{0,3},{1,0},{2,1},{3,2},{4,7},{5,4},{6,5},{7,6},{8,11},{9,8},{10,9... | collective-permute-start | bytes 1179656 | tf_op jit(solution)/shard_map/ppermute | solution.py:370
  106.7 13.3 %collective-permute-start.6 = (bf16[96,2048]{1,0:T(8,128)(2,1)S(1)}, bf16[96,2048]{1,0:T(8,128)(2,1)S(1)}, u32[]{:S(2)}, u32[]{:S(2)}) collective-permute-start(bf16[96,2048]{1,0:T(8,128)(2,1)S(1)} %get-tuple-element.64), channel_id=1, source_target_pairs={{0,3},{1,0},{2,1},{3,2},{4,7},{5,4},{6,5},{7,6},{8,11},{9,8},{10,9... | collective-permute-start | bytes 1179656 | tf_op jit(solution)/shard_map/ppermute | solution.py:370
  108.6 12.3 %collective-permute-start.5 = (bf16[96,2048]{1,0:T(8,128)(2,1)S(1)}, bf16[96,2048]{1,0:T(8,128)(2,1)S(1)}, u32[]{:S(2)}, u32[]{:S(2)}) collective-permute-start(bf16[96,2048]{1,0:T(8,128)(2,1)S(1)} %shard_map.272), channel_id=1, source_target_pairs={{0,1},{1,2},{2,3},{3,0},{4,5},{5,6},{6,7},{7,4},{8,9},{9,10},{10,1... | collective-permute-start | bytes 1179656 | tf_op jit(solution)/shard_map/ppermute | solution.py:370
  110.4 18.9 %collective-permute-start.7 = (bf16[96,2048]{1,0:T(8,128)(2,1)S(1)}, bf16[96,2048]{1,0:T(8,128)(2,1)S(1)}, u32[]{:S(2)}, u32[]{:S(2)}) collective-permute-start(bf16[96,2048]{1,0:T(8,128)(2,1)S(1)} %get-tuple-element.68), channel_id=1, source_target_pairs={{0,1},{1,2},{2,3},{3,0},{4,5},{5,6},{6,7},{7,4},{8,9},{9,10},{10,1... | collective-permute-start | bytes 1179656 | tf_op jit(solution)/shard_map/ppermute | solution.py:370
  110.7 18.6 %collective-permute-start.9 = (bf16[96,2048]{1,0:T(8,128)(2,1)S(1)}, bf16[96,2048]{1,0:T(8,128)(2,1)S(1)}, u32[]{:S(2)}, u32[]{:S(2)}) collective-permute-start(bf16[96,2048]{1,0:T(8,128)(2,1)S(1)} %shard_map.274), channel_id=1, source_target_pairs={{0,3},{1,0},{2,1},{3,2},{4,7},{5,4},{6,5},{7,6},{8,11},{9,8},{10,9... | collective-permute-start | bytes 1179656 | tf_op jit(solution)/shard_map/ppermute | solution.py:370
  121.3 14.6 %collective-permute-start.10 = (bf16[96,2048]{1,0:T(8,128)(2,1)S(1)}, bf16[96,2048]{1,0:T(8,128)(2,1)S(1)}, u32[]{:S(2)}, u32[]{:S(2)}) collective-permute-start(bf16[96,2048]{1,0:T(8,128)(2,1)S(1)} %get-tuple-element.66.refs_0_), channel_id=1, source_target_pairs={{0,1},{1,2},{2,3},{3,0},{4,5},{5,6},{6,7},{7,4},{8,9},{9,10},{10,1... | collective-permute-start | bytes 1179656 | tf_op jit(solution)/shard_map/ppermute | solution.py:370
  130.4 9.0 %collective-permute-start.13 = (bf16[96,2048]{1,0:T(8,128)(2,1)S(1)}, bf16[96,2048]{1,0:T(8,128)(2,1)S(1)}, u32[]{:S(2)}, u32[]{:S(2)}) collective-permute-start(bf16[96,2048]{1,0:T(8,128)(2,1)S(1)} %get-tuple-element.71.refs_1_), channel_id=1, source_target_pairs={{0,3},{1,0},{2,1},{3,2},{4,7},{5,4},{6,5},{7,6},{8,11},{9,8},{10,9... | collective-permute-start | bytes 1179656 | tf_op jit(solution)/shard_map/ppermute | solution.py:370
  135.9 12.5 %collective-permute-start.14 = (bf16[96,2048]{1,0:T(8,128)(2,1)S(1)}, bf16[96,2048]{1,0:T(8,128)(2,1)S(1)}, u32[]{:S(2)}, u32[]{:S(2)}) collective-permute-start(bf16[96,2048]{1,0:T(8,128)(2,1)S(1)} %collective-permute-done.10.refs_0_), channel_id=1, source_target_pairs={{0,1},{1,2},{2,3},{3,0},{4,5},{5,6},{6,7},{7,4},{8,9},{9,10},{10,1... | collective-permute-start | bytes 1179656 | tf_op jit(solution)/shard_map/ppermute | solution.py:370
  139.5 13.2 %collective-permute-start.15 = (bf16[96,2048]{1,0:T(8,128)(2,1)S(1)}, bf16[96,2048]{1,0:T(8,128)(2,1)S(1)}, u32[]{:S(2)}, u32[]{:S(2)}) collective-permute-start(bf16[96,2048]{1,0:T(8,128)(2,1)S(1)} %collective-permute-done.13.refs_3_), channel_id=1, source_target_pairs={{0,3},{1,0},{2,1},{3,2},{4,7},{5,4},{6,5},{7,6},{8,11},{9,8},{10,9... | collective-permute-start | bytes 1179656 | tf_op jit(solution)/shard_map/ppermute | solution.py:370
  139.5 21.5 %collective-permute-start.11 = (bf16[96,2048]{1,0:T(8,128)(2,1)S(1)}, bf16[96,2048]{1,0:T(8,128)(2,1)S(1)}, u32[]{:S(2)}, u32[]{:S(2)}) collective-permute-start(bf16[96,2048]{1,0:T(8,128)(2,1)S(1)} %get-tuple-element.71.refs_1_), channel_id=1, source_target_pairs={{0,1},{1,2},{2,3},{3,0},{4,5},{5,6},{6,7},{7,4},{8,9},{9,10},{10,1... | collective-permute-start | bytes 1179656 | tf_op jit(solution)/shard_map/ppermute | solution.py:370
  142.7 18.3 %collective-permute-start.12 = (bf16[96,2048]{1,0:T(8,128)(2,1)S(1)}, bf16[96,2048]{1,0:T(8,128)(2,1)S(1)}, u32[]{:S(2)}, u32[]{:S(2)}) collective-permute-start(bf16[96,2048]{1,0:T(8,128)(2,1)S(1)} %get-tuple-element.66.refs_0_), channel_id=1, source_target_pairs={{0,3},{1,0},{2,1},{3,2},{4,7},{5,4},{6,5},{7,6},{8,11},{9,8},{10,9... | collective-permute-start | bytes 1179656 | tf_op jit(solution)/shard_map/ppermute | solution.py:370
  158.8 12.9 %collective-permute-start.16 = (bf16[96,2048]{1,0:T(8,128)(2,1)S(1)}, bf16[96,2048]{1,0:T(8,128)(2,1)S(1)}, u32[]{:S(2)}, u32[]{:S(2)}) collective-permute-start(bf16[96,2048]{1,0:T(8,128)(2,1)S(1)} %get-tuple-element.75), channel_id=1, source_target_pairs={{0,1},{1,2},{2,3},{3,0},{4,5},{5,6},{6,7},{7,4},{8,9},{9,10},{10,1... | collective-permute-start | bytes 1179656 | tf_op jit(solution)/shard_map/ppermute | solution.py:370
  160.1 13.0 %collective-permute-start.20 = (bf16[96,2048]{1,0:T(8,128)(2,1)S(1)}, bf16[96,2048]{1,0:T(8,128)(2,1)S(1)}, u32[]{:S(2)}, u32[]{:S(2)}) collective-permute-start(bf16[96,2048]{1,0:T(8,128)(2,1)S(1)} %get-tuple-element.81), channel_id=1, source_target_pairs={{0,3},{1,0},{2,1},{3,2},{4,7},{5,4},{6,5},{7,6},{8,11},{9,8},{10,9... | collective-permute-start | bytes 1179656 | tf_op jit(solution)/shard_map/ppermute | solution.py:370
  168.4 13.3 %collective-permute-start.18 = (bf16[96,2048]{1,0:T(8,128)(2,1)S(1)}, bf16[96,2048]{1,0:T(8,128)(2,1)S(1)}, u32[]{:S(2)}, u32[]{:S(2)}) collective-permute-start(bf16[96,2048]{1,0:T(8,128)(2,1)S(1)} %get-tuple-element.76), channel_id=1, source_target_pairs={{0,3},{1,0},{2,1},{3,2},{4,7},{5,4},{6,5},{7,6},{8,11},{9,8},{10,9... | collective-permute-start | bytes 1179656 | tf_op jit(solution)/shard_map/ppermute | solution.py:370
  168.5 13.2 %collective-permute-start.19 = (bf16[96,2048]{1,0:T(8,128)(2,1)S(1)}, bf16[96,2048]{1,0:T(8,128)(2,1)S(1)}, u32[]{:S(2)}, u32[]{:S(2)}) collective-permute-start(bf16[96,2048]{1,0:T(8,128)(2,1)S(1)} %get-tuple-element.79), channel_id=1, source_target_pairs={{0,1},{1,2},{2,3},{3,0},{4,5},{5,6},{6,7},{7,4},{8,9},{9,10},{10,1... | collective-permute-start | bytes 1179656 | tf_op jit(solution)/shard_map/ppermute | solution.py:370
  171.8 11.7 %collective-permute-start.17 = (bf16[96,2048]{1,0:T(8,128)(2,1)S(1)}, bf16[96,2048]{1,0:T(8,128)(2,1)S(1)}, u32[]{:S(2)}, u32[]{:S(2)}) collective-permute-start(bf16[96,2048]{1,0:T(8,128)(2,1)S(1)} %shard_map.279), channel_id=1, source_target_pairs={{0,1},{1,2},{2,3},{3,0},{4,5},{5,6},{6,7},{7,4},{8,9},{9,10},{10,1... | collective-permute-start | bytes 1179656 | tf_op jit(solution)/shard_map/ppermute | solution.py:370
  173.2 12.7 %copy-start.5 = (bf16[96,2048]{1,0:T(8,128)(2,1)S(1)}, bf16[96,2048]{1,0:T(8,128)(2,1)}, u32[]{:S(2)}) copy-start(bf16[96,2048]{1,0:T(8,128)(2,1)} %copy-done.4) | copy-start | bytes 1179652
  173.3 12.7 %collective-permute-start.21 = (bf16[96,2048]{1,0:T(8,128)(2,1)S(1)}, bf16[96,2048]{1,0:T(8,128)(2,1)S(1)}, u32[]{:S(2)}, u32[]{:S(2)}) collective-permute-start(bf16[96,2048]{1,0:T(8,128)(2,1)S(1)} %shard_map.280), channel_id=1, source_target_pairs={{0,3},{1,0},{2,1},{3,2},{4,7},{5,4},{6,5},{7,6},{8,11},{9,8},{10,9... | collective-permute-start | bytes 1179656 | tf_op jit(solution)/shard_map/ppermute | solution.py:370
  (6 other events, 30.1 us)
Sparse Core Ops, SparseCore 0:
  44.8 90.6 all-gather.1
